TPU v7x, 32 devices: a whole 2x2x4 slice. The times are simulated.
32 devices in a mesh: dp: 4 (over y, x), kv: 4 (over z), tp: 2 (over core).
Axes of the slice: x: 2, y: 2, z: 4, core: 2. Of those that a mesh axis runs over, the one named last changes fastest.
Arguments:
- tokens: bfloat16 [16, 24, 2048], P('dp'), may hold values from -6 to 6
- norm_gain: bfloat16 [2048], replicated, may hold values from 0.099609375 to 1.8984375
- w_query: bfloat16 [2048, 1024], P('kv', 'tp'), may hold values from -0.125 to 0.125
- w_key: bfloat16 [2048, 1024], P('kv', 'tp'), may hold values from -0.03125 to 0.03125
- w_value: bfloat16 [2048, 1024], P('kv', 'tp'), may hold values from -0.03125 to 0.03125
- w_forget: bfloat16 [2048, 16], P('kv', 'tp'), may hold values from -0.125 to 0.125
- forget_bias: float32 [16], P('tp'), may hold values from 0 to 4
- head_gain: bfloat16 [1024], P('tp'), may hold values from 0.099609375 to 1.8984375
- w_out: bfloat16 [1024, 2048], P('tp', 'kv'), may hold values from -0.1875 to 0.1875
- cache_keys: bfloat16 [16, 1024, 1024], P('dp', 'kv', 'tp'), may hold values from -480 to 480
- cache_values: bfloat16 [16, 1024, 1024], P('dp', 'kv', 'tp'), may hold values from -1.5 to 1.5
- cache_gates: float32 [16, 16, 1024], P('dp', 'tp', 'kv'), may hold values from -128 to 0, as said below
- lengths: int32 [16], P('dp'), may hold values from 512 to 975
- accepted: int32 [16], P('dp'), may hold values from 0 to 23
- parents: int32 [16, 24], P('dp'), may hold values from -1 to 22, as said below
Outputs:
- mixed: float32 [16, 24, 2048], P('dp', None, ('kv', 'tp'))
- keys_out: bfloat16 [16, 1024, 1024], P('dp', 'kv', 'tp')
- values_out: bfloat16 [16, 1024, 1024], P('dp', 'kv', 'tp')
- gates_out: float32 [16, 16, 1024], P('dp', 'tp', 'kv')
Inputs may be any that keep to these rules, and one draw needn't show every extreme that they name: parents[b, 0] = -1 and 0 <= parents[b, j] < j for every later proposal j. `cache_gates`: nonincreasing along the positions of each sequence and head.
All inputs are finite; a program needn't handle non-finite values.
Results may differ from a plain program's by a relative error of at most 0.008.
Values may be sent and summed in bfloat16 or wider, within the bound.
A program may use at most 64 MiB of HBM per device.

v0:
```python
import jax
import jax.numpy as jnp
from jax import lax
from jax.sharding import PartitionSpec as P

NEG_LARGE = -1e30
EPSILON = 1e-06


def joined_2(value, axis, join):
    pieces = jax.tree.map(lambda part: lax.all_gather(part, axis), value)
    head = jax.tree.map(lambda part: part[0], pieces)
    tail = jax.tree.map(lambda part: part[1:], pieces)
    total, _ = lax.scan(lambda total, piece: (join(total, piece), None), head, tail)
    return total


def ancestry(parents):
    prop_count = parents.shape[1]
    indices = jnp.arange(prop_count, dtype=jnp.int32)
    linked = (parents[:, :, None] == indices[None, None, :]).astype(jnp.float32)
    linked = linked + (indices[:, None] == indices[None, :]).astype(jnp.float32)[None]
    for repeat in range(prop_count.bit_length()):
        linked = jnp.minimum(
            jnp.einsum("bij,bjk->bik", linked, linked, precision=lax.Precision.HIGHEST), 1.0
        )
    return linked


def merge_pair(first_part, second_part):
    highest = jnp.maximum(first_part[0], second_part[0])
    scale_first = jnp.exp(first_part[0] - highest)
    scale_second = jnp.exp(second_part[0] - highest)
    seq_count, prop_count, head_count = highest.shape
    outer_first = (
        first_part[2].reshape(seq_count, prop_count, head_count, -1) * scale_first[..., None]
    )
    outer_second = (
        second_part[2].reshape(seq_count, prop_count, head_count, -1) * scale_second[..., None]
    )
    joined = (outer_first + outer_second).reshape(seq_count, prop_count, -1)
    return (highest, first_part[1] * scale_first + second_part[1] * scale_second, joined)


def local(
    tokens,
    norm_gain,
    w_query,
    w_key,
    w_value,
    w_forget,
    forget_bias,
    head_gain,
    w_out,
    cache_keys,
    cache_values,
    cache_gates,
    lengths,
    accepted,
    parents,
):
    seq_count, prop_count, model_width = tokens.shape
    span_rows = cache_keys.shape[1]
    head_count = cache_gates.shape[1]
    head_size = cache_keys.shape[2] // head_count
    scale = head_size ** (-0.5)
    start_pos = lax.axis_index("kv") * span_rows
    positions = start_pos + jnp.arange(span_rows, dtype=jnp.int32)
    valid_len = lengths + accepted
    flat_rows = tokens.reshape(seq_count * prop_count, model_width).astype(jnp.float32)
    normed = (
        flat_rows
        * lax.rsqrt(jnp.mean(flat_rows * flat_rows, axis=1, keepdims=True) + EPSILON)
        * norm_gain.astype(jnp.float32)
    ).astype(jnp.bfloat16)
    picked = (positions[None, :] == (valid_len - 1)[:, None]).astype(jnp.float32)
    last_part = jnp.sum(cache_gates * picked[:, None, :], axis=2)
    row_count = w_query.shape[0]
    own_columns = lax.dynamic_slice_in_dim(normed, lax.axis_index("kv") * row_count, row_count, 1)
    query_part = jnp.dot(own_columns, w_query, preferred_element_type=jnp.float32)
    key_part = jnp.dot(own_columns, w_key, preferred_element_type=jnp.float32)
    value_part = jnp.dot(own_columns, w_value, preferred_element_type=jnp.float32)
    gate_part = jnp.dot(own_columns, w_forget, preferred_element_type=jnp.float32)
    query, fresh_keys, fresh_values, gate_pre, last_gate = lax.psum(
        (query_part, key_part, value_part, gate_part, last_part), "kv"
    )
    query = query.astype(jnp.bfloat16).reshape(seq_count, prop_count, head_count, head_size)
    fresh_keys = fresh_keys.astype(jnp.bfloat16).reshape(
        seq_count, prop_count, head_count, head_size
    )
    fresh_values = fresh_values.astype(jnp.bfloat16).reshape(
        seq_count, prop_count, head_count, head_size
    )
    log_gate = jax.nn.log_sigmoid(gate_pre + forget_bias).reshape(seq_count, prop_count, head_count)
    link = ancestry(parents)
    climb = jnp.einsum("bia,bah->bih", link, log_gate, precision=lax.Precision.HIGHEST)
    stored_keys = cache_keys.reshape(seq_count, span_rows, head_count, head_size)
    stored_values = cache_values.reshape(seq_count, span_rows, head_count, head_size)
    scores = (
        jnp.einsum("bphd,bchd->bphc", query, stored_keys, preferred_element_type=jnp.float32)
        * scale
    )
    scores = scores + (last_gate[:, None, :] + climb)[..., None] - cache_gates[:, None]
    seen = (positions[None, :] < valid_len[:, None])[:, None, None, :]
    highest = jnp.max(jnp.where(seen, scores, NEG_LARGE), axis=3)
    weights = jnp.where(seen, jnp.exp(scores - highest[..., None]), 0.0)
    normalizer = jnp.sum(weights, axis=3)
    weighted = jnp.einsum(
        "bphc,bchd->bphd",
        weights.astype(jnp.bfloat16),
        stored_values,
        preferred_element_type=jnp.float32,
    )
    highest, normalizer, weighted = joined_2(
        (highest, normalizer, weighted.reshape(seq_count, prop_count, head_count * head_size)),
        "kv",
        merge_pair,
    )
    near_scores = (
        jnp.einsum("bphd,bahd->bpha", query, fresh_keys, preferred_element_type=jnp.float32) * scale
    )
    near_scores = near_scores + climb[..., None] - jnp.transpose(climb, (0, 2, 1))[:, None]
    linked = (link > 0.5)[:, :, None, :]
    near_high = jnp.max(jnp.where(linked, near_scores, NEG_LARGE), axis=3)
    overall = jnp.maximum(highest, near_high)
    carried = jnp.exp(highest - overall)
    near_weights = jnp.where(linked, jnp.exp(near_scores - overall[..., None]), 0.0)
    normalizer = normalizer * carried + jnp.sum(near_weights, axis=3)
    attended = weighted.reshape(seq_count, prop_count, head_count, head_size) * carried[..., None]
    attended = attended + jnp.einsum(
        "bpha,bahd->bphd",
        near_weights.astype(jnp.bfloat16),
        fresh_values,
        preferred_element_type=jnp.float32,
    )
    attended = attended / normalizer[..., None]
    gain_rows = head_gain.astype(jnp.float32).reshape(head_count, head_size)
    heads_out = (
        (
            attended
            * lax.rsqrt(jnp.mean(attended * attended, axis=3, keepdims=True) + EPSILON)
            * gain_rows
        )
        .astype(jnp.bfloat16)
        .reshape(seq_count * prop_count, head_count * head_size)
    )
    partial_sum = jnp.dot(heads_out, w_out, preferred_element_type=jnp.float32)
    summed = lax.psum_scatter(partial_sum, "tp", scatter_dimension=1, tiled=True)
    mixed = summed.reshape(seq_count, prop_count, -1)
    offsets = positions[None, :, None] - valid_len[:, None, None]
    placed = offsets == jnp.arange(prop_count, dtype=jnp.int32)[None, None, :]
    landed = jnp.any(placed, axis=2)
    placed_low = placed.astype(jnp.bfloat16)
    written_keys = jnp.einsum(
        "bcj,bjx->bcx",
        placed_low,
        fresh_keys.reshape(seq_count, prop_count, -1),
        preferred_element_type=jnp.float32,
    ).astype(jnp.bfloat16)
    written_values = jnp.einsum(
        "bcj,bjx->bcx",
        placed_low,
        fresh_values.reshape(seq_count, prop_count, -1),
        preferred_element_type=jnp.float32,
    ).astype(jnp.bfloat16)
    keys_out = jnp.where(landed[..., None], written_keys, cache_keys)
    values_out = jnp.where(landed[..., None], written_values, cache_values)
    new_gates = last_gate[:, :, None] + jnp.transpose(climb, (0, 2, 1))
    written_gates = jnp.einsum(
        "bcj,bhj->bhc", placed.astype(jnp.float32), new_gates, precision=lax.Precision.HIGHEST
    )
    gates_out = jnp.where(landed[:, None, :], written_gates, cache_gates)
    return (mixed, keys_out, values_out, gates_out)


def solution(mesh):
    placed = (
        P("dp", None, None),
        P(),
        P("kv", "tp"),
        P("kv", "tp"),
        P("kv", "tp"),
        P("kv", "tp"),
        P("tp"),
        P("tp"),
        P("tp", "kv"),
        P("dp", "kv", "tp"),
        P("dp", "kv", "tp"),
        P("dp", "tp", "kv"),
        P("dp"),
        P("dp"),
        P("dp", None),
    )
    return jax.shard_map(
        local,
        mesh=mesh,
        in_specs=placed,
        out_specs=(
            P("dp", None, ("kv", "tp")),
            P("dp", "kv", "tp"),
            P("dp", "kv", "tp"),
            P("dp", "tp", "kv"),
        ),
        check_vma=False,
    )
```

profile of v0, /device:TPU:0, one launch (start us, length us, event | category | flops | bytes accessed | tf_op | source)
XLA Modules:
  0.0 120.9 jit_solution(18066917370069135501)
XLA Ops:
  7.2 1.1 bitcast_convert_fusion
  10.2 0.5 copy-done.15
  10.8 34.3 %all-reduce.2 = (f32[96,8]{0,1:T(8,128)S(1)}, f32[4,8]{1,0:T(4,128)S(1)}, bf16[96,512]{1,0:T(8,128)(2,1)S(1)}, bf16[96,512]{1,0:T(8,128)(2,1)}, bf16[96,512]{1,0:T(8,128)(2,1)S(1)}) all-reduce(f32[96,8]{0,1:T(8,128)S(1)} %fusion.50, f32[4,8]{1,0:T(4,128)S(1)} %multiply_reduce_fusion.2, ...), channel_id=1, replica_groups=mesh['dp'=4,'kv'=4,'tp'=2] {'kv'}, use_global_device_ids=true, to_apply=%region_4.0 | all-reduce | flops 148256 | bytes 891136 | tf_op jit(solution)/shard_map/psum | solution.py:84
  46.2 0.8 broadcast_compare_fusion
  47.2 1.3 %copy.46 = bf16[4,256,512]{1,2,0:T(8,128)(2,1)} copy(bf16[4,256,512]{2,1,0:T(8,128)(2,1)S(1)} %copy-done.1) | data formatting | bytes 2097152 | tf_op args[9]
  48.5 1.3 %copy.49 = bf16[4,256,512]{1,2,0:T(8,128)(2,1)} copy(bf16[4,256,512]{2,1,0:T(8,128)(2,1)S(1)} %copy-done.2) | data formatting | bytes 2097152 | tf_op args[10]
  49.8 0.8 broadcast_add_fusion
  50.6 1.7 %select_reduce_fusion = (f32[4,24,8]{1,2,0:T(8,128)S(1)}, f32[4,24,8,256]{3,1,2,0:T(8,128)S(1)}) fusion(pred[4,256]{1,0:T(4,128)(4,1)S(1)} %get-tuple-element.73, f32[4,8,256]{2,1,0:T(8,128)S(1)} %copy-done.10, f32[4,24,8]{1,2,0:T(8,128)S(1)} %get-tuple-element.75, bf16[4,256,8,64]{1,3,2,0:T(8,128)(2,1)} %bitcast.90, bf16[4,24,8,64]{3,2,1,0:T(8,128)(2,1)S(1)} %reshape.192), kind=kOutput, calls=%fused_computation.31 | convolution fusion | flops 26148096 | bytes 1973248 | tf_op jit(solution)/shard_map/bphd,bchd->bphc/dot_general | solution.py:100
  53.0 17.6 %all_gather.19 = f32[4,4,24,512]{3,2,1,0:T(8,128)S(1)} all-gather(f32[1,4,24,512]{3,2,1,0:T(8,128)S(1)} %all_gather_reshape.3), channel_id=1, replica_groups=mesh['dp'=4,'kv'=4,'tp'=2] {'kv'}, dimensions={0}, use_global_device_ids=true | all-gather | bytes 983040 | tf_op jit(solution)/shard_map/all_gather | solution.py:11
  71.0 13.3 %all-gather.1 = f32[16,24,8]{1,2,0:T(8,128)S(1)} all-gather(f32[4,24,8]{1,2,0:T(8,128)S(1)} %fusion.14), channel_id=3, replica_groups=mesh['dp'=4,'kv'=4,'tp'=2] {'kv'}, dimensions={0}, use_global_device_ids=true | all-gather | bytes 15360 | tf_op jit(solution)/shard_map/all_gather | solution.py:11
  84.2 13.1 %all-gather = f32[16,24,8]{1,2,0:T(8,128)S(1)} all-gather(f32[4,24,8]{1,2,0:T(8,128)S(1)} %get-tuple-element.77), channel_id=2, replica_groups=mesh['dp'=4,'kv'=4,'tp'=2] {'kv'}, dimensions={0}, use_global_device_ids=true | all-gather | bytes 15360 | tf_op jit(solution)/shard_map/all_gather | solution.py:11
  97.4 0.6 slice.31
  98.0 4.8 %while.14 = (s32[]{:T(128)}, f32[4,24,8]{1,2,0:T(8,128)S(1)}, f32[4,24,8]{1,2,0:T(8,128)S(1)}, f32[4,24,512]{2,1,0:T(8,128)S(1)}, f32[3,4,24,8]{2,3,1,0:T(8,128)...) while((s32[]{:T(128)}, f32[4,24,8]{1,2,0:T(8,128)S(1)}, ...), condition=%wide.region_8.9_spmd, body=%wide.region_7.8_spmd.sunk | while | flops 152066 | bytes 2205789 | solution.py:14
  98.0 0.7 fusion.79
  99.6 0.7 fusion.79
  101.2 0.7 fusion.79
  103.0 1.1 reshape.197
  104.0 0.8 copy.51
  105.4 0.5 multiply_reduce_fusion.1
  107.0 0.9 fusion.53
  108.1 1.5 %fusion.3 = bf16[4,256,512]{2,1,0:T(8,128)(2,1)} fusion(bf16[4,256,512]{2,1,0:T(8,128)(2,1)S(1)} %copy-done.1, bf16[4,24,512]{2,1,0:T(8,128)(2,1)S(1)} %bitcast.92, pred[4,256]{1,0:T(4,128)(4,1)S(1)} %fusion.31, s32[4,256]{1,0:T(4,128)S(1)} %broadcast_subtract_fusion), kind=kOutput, calls=%fused_computation.10 | convolution fusion | flops 26238976 | bytes 2200576 | tf_op jit(solution)/shard_map/bcj,bjx->bcx/dot_general | solution.py:154
  109.5 0.8 convolution_select_fusion
  110.4 1.5 %fusion.4 = bf16[4,256,512]{2,1,0:T(8,128)(2,1)} fusion(bf16[4,256,512]{2,1,0:T(8,128)(2,1)S(1)} %copy-done.3, bf16[4,24,512]{2,1,0:T(8,128)(2,1)S(1)} %bitcast.91, pred[4,256]{1,0:T(4,128)(4,1)S(1)} %fusion.31, s32[4,256]{1,0:T(4,128)S(1)} %broadcast_subtract_fusion), kind=kOutput, calls=%fused_computation.11 | convolution fusion | flops 26238976 | bytes 2200576 | tf_op jit(solution)/shard_map/bcj,bjx->bcx/dot_general | solution.py:160
  111.8 2.2 %reduce-scatter.2.cloned.1.call-done = f32[96,256]{1,0:T(8,128)} async-done(((f32[96,512]{1,0:T(8,128)}), f32[96,256]{1,0:T(8,128)}) %reduce-scatter.2.cloned.1.call-update) | async-done | bytes 98320 | tf_op jit(solution)/shard_map/reduce_scatter | solution.py:148
  (115 shorter events, 8.5 us)
Async XLA Ops:
  7.2 1.7 %copy-start = (bf16[512,512]{1,0:T(8,128)(2,1)S(1)}, bf16[512,512]{1,0:T(8,128)(2,1)}, u32[]{:S(2)}) copy-start(bf16[512,512]{1,0:T(8,128)(2,1)} %param.19) | copy-start | bytes 1572868
  7.2 1.2 copy-start.5
  7.2 1.5 %copy-start.21 = (bf16[2048]{0:T(1024)(128)(2,1)S(1)}, bf16[2048]{0:T(1024)(128)(2,1)}, u32[]{:S(2)}) copy-start(bf16[2048]{0:T(1024)(128)(2,1)} %param.18) | copy-start | bytes 12292
  7.2 106.8 %reduce-scatter.2.cloned.1.call-start = ((), (), s32[]{:S(2)}) async-start(), calls=%async_computation.1 | async-start | bytes 294912 | tf_op jit(solution)/shard_map/reduce_scatter | solution.py:148
  8.4 1.1 copy-start.6
  8.6 1.1 copy-start.7
  8.9 1.1 copy-start.12
  9.5 0.7 copy-start.23
  9.5 0.7 copy-start.24
  9.5 1.2 %copy-start.10 = (f32[4,8,256]{2,1,0:T(8,128)S(1)}, f32[4,8,256]{2,1,0:T(8,128)}, u32[]{:S(2)}) copy-start(f32[4,8,256]{2,1,0:T(8,128)} %param.28) | copy-start | bytes 98308
  9.5 35.6 %copy-start.22 = (f32[8]{0:T(128)S(1)}, f32[8]{0:T(128)}, u32[]{:S(2)}) copy-start(f32[8]{0:T(128)} %param.23) | copy-start | bytes 100
  9.5 35.8 %copy-start.19 = (s32[4,24]{1,0:T(4,128)S(1)}, s32[4,24]{1,0:T(4,128)}, u32[]{:S(2)}) copy-start(s32[4,24]{1,0:T(4,128)} %param.31) | copy-start | bytes 1156
  9.9 37.3 %copy-start.1 = (bf16[4,256,512]{2,1,0:T(8,128)(2,1)S(1)}, bf16[4,256,512]{2,1,0:T(8,128)(2,1)}, u32[]{:S(2)}) copy-start(bf16[4,256,512]{2,1,0:T(8,128)(2,1)} %param.26) | copy-start | bytes 3145732
  10.2 36.9 %copy-start.17 = (s32[256]{0:T(256)}, s32[256]{0:T(256)S(1)}, u32[]{:S(2)}) copy-start(s32[256]{0:T(256)S(1)} %iota_add_fusion) | copy-start | bytes 3076
  45.1 4.8 %copy-start.13 = (f32[4,8]{1,0:T(4,128)}, f32[4,8]{1,0:T(4,128)S(1)}, u32[]{:S(2)}) copy-start(f32[4,8]{1,0:T(4,128)S(1)} %get-tuple-element.61) | copy-start | bytes 388
  47.2 1.3 %copy-start.2 = (bf16[4,256,512]{2,1,0:T(8,128)(2,1)S(1)}, bf16[4,256,512]{2,1,0:T(8,128)(2,1)}, u32[]{:S(2)}) copy-start(bf16[4,256,512]{2,1,0:T(8,128)(2,1)} %param.27) | copy-start | bytes 3145732
  50.6 1.7 %copy-start.4 = (bf16[4,256,512]{1,2,0:T(8,128)(2,1)S(1)}, bf16[4,256,512]{1,2,0:T(8,128)(2,1)}, u32[]{:S(2)}) copy-start(bf16[4,256,512]{1,2,0:T(8,128)(2,1)} %copy.49) | copy-start | bytes 3145732
  102.8 2.2 %copy-start.11 = (f32[4,24,8]{1,2,0:T(8,128)S(1)}, f32[4,24,8]{1,2,0:T(8,128)}, u32[]{:S(2)}) copy-start(f32[4,24,8]{1,2,0:T(8,128)} %get-tuple-element.76) | copy-start | bytes 9220
  106.0 1.0 copy-start.8
  106.2 1.7 %copy-start.16 = (s32[4]{0:T(128)S(1)}, s32[4]{0:T(128)}, u32[]{:S(2)}) copy-start(s32[4]{0:T(128)} %copy-done.15) | copy-start | bytes 52
  106.2 1.7 %copy-start.18 = (s32[256]{0:T(256)S(1)}, s32[256]{0:T(256)}, u32[]{:S(2)}) copy-start(s32[256]{0:T(256)} %copy-done.17) | copy-start | bytes 3076
  106.2 1.9 %copy-start.9 = (bf16[96,512]{1,0:T(8,128)(2,1)S(1)}, bf16[96,512]{1,0:T(8,128)(2,1)}, u32[]{:S(2)}) copy-start(bf16[96,512]{1,0:T(8,128)(2,1)} %get-tuple-element.63) | copy-start | bytes 294916
  108.1 1.5 %copy-start.14 = (f32[4,8]{1,0:T(4,128)S(1)}, f32[4,8]{1,0:T(4,128)}, u32[]{:S(2)}) copy-start(f32[4,8]{1,0:T(4,128)} %copy-done.13) | copy-start | bytes 388
  108.1 2.3 %copy-start.3 = (bf16[4,256,512]{2,1,0:T(8,128)(2,1)S(1)}, bf16[4,256,512]{2,1,0:T(8,128)(2,1)}, u32[]{:S(2)}) copy-start(bf16[4,256,512]{2,1,0:T(8,128)(2,1)} %param.27) | copy-start | bytes 3145732
  (2 other events, 1.2 us)
Sparse Core Ops, SparseCore 0:
  108.0 5.9 reduce-scatter.1
where the time goes:
time: 121 us
  blocking collectives  78.2 us (65%)
  between operations  14.5 us (12%)
  matrix products  10.9 us (9%)
  local copies, waits for them, and re-layouts  10.1 us (8%)
  other arithmetic  4.89 us (4%)
  waiting for transfers between devices  2.2 us (2%)
    all_gather x3, blocking collectives, joined_2(): pieces = jax.tree.map(lambda part: lax.all_gather(part, axis), value)  43.9 us
    psum x1, blocking collectives, local(): lax.psum((query_part, key_part, value_part, gate_part, last_part), 'kv')  34.3 us
    unnamed x52, local copies, waits for them, and re-layouts  4.17 us
  transfers between devices with their start and end apart: 1, of which 1 were waited for; matrix products, arithmetic and copies ran while one was open for 3% of the time, Pallas kernels for 0%

commit v1 on v0

--- a/solution.py
+++ b/solution.py
@@ -1,6 +1,10 @@
+import functools
+
 import jax
 import jax.numpy as jnp
 from jax import lax
+from jax.experimental import pallas as pl
+from jax.experimental.pallas import tpu as pltpu
 from jax.sharding import PartitionSpec as P
 
 NEG_LARGE = -1e30
@@ -173,6 +177,513 @@
     return (mixed, keys_out, values_out, gates_out)
 
 
+HIGHEST = lax.Precision.HIGHEST
+MESH = pl.DeviceIdType.MESH
+LANES = 128
+
+
+def dot_rows(left, right, precision=None):
+    return lax.dot_general(
+        left,
+        right,
+        (((1,), (1,)), ((), ())),
+        precision=precision,
+        preferred_element_type=jnp.float32,
+    )
+
+
+def dot_plain(left, right, precision=None):
+    return jnp.dot(left, right, precision=precision, preferred_element_type=jnp.float32)
+
+
+def exchange_kernel(
+    kv_count,
+    head_count,
+    lengths_ref,
+    accepted_ref,
+    tokens_hbm,
+    gain_hbm,
+    wq_hbm,
+    wk_hbm,
+    wv_hbm,
+    wf_hbm,
+    bias_hbm,
+    head_gain_hbm,
+    wo_hbm,
+    keys_hbm,
+    values_hbm,
+    gates_hbm,
+    parents_hbm,
+    mixed_out,
+    fresh_out,
+    fresh_gates_out,
+    tokens_ref,
+    gain_ref,
+    wq_ref,
+    wk_ref,
+    wv_ref,
+    wf_ref,
+    bias_ref,
+    head_gain_ref,
+    wo_ref,
+    keys_ref,
+    values_ref,
+    gates_ref,
+    parents_ref,
+    q_send,
+    q_recv,
+    q_all,
+    kv_send,
+    kv_recv,
+    kv_all,
+    g_send,
+    g_recv,
+    g_all,
+    w_send,
+    w_recv,
+    st_send,
+    st_recv,
+    h_all,
+    o_send,
+    o_recv,
+    load_sem,
+    send_sem,
+    recv_sem,
+    pair_sem,
+):
+    dp, me, tp = lax.axis_index("dp"), lax.axis_index("kv"), lax.axis_index("tp")
+    seq_count, prop, _ = tokens_ref.shape
+    depth, width = wq_ref.shape
+    span = keys_ref.shape[1]
+    head_size = width // head_count
+    scale = head_size ** (-0.5)
+    rows_all = head_count * prop
+    half = wo_ref.shape[1] // 2
+    offsets = range(1, kv_count)
+
+    sources = (
+        (tokens_hbm, tokens_ref),
+        (gain_hbm, gain_ref),
+        (wq_hbm, wq_ref),
+        (wk_hbm, wk_ref),
+        (wv_hbm, wv_ref),
+        (wf_hbm, wf_ref),
+        (gates_hbm, gates_ref),
+        (keys_hbm, keys_ref),
+        (values_hbm, values_ref),
+        (parents_hbm, parents_ref),
+        (bias_hbm, bias_ref),
+        (head_gain_hbm, head_gain_ref),
+        (wo_hbm, wo_ref),
+    )
+    loads = {}
+    for at, (source, target) in enumerate(sources):
+        copy = pltpu.make_async_copy(source, target, load_sem.at[at])
+        copy.start()
+        loads[id(target)] = copy
+
+    def loaded(*refs):
+        for ref in refs:
+            loads[id(ref)].wait()
+
+    barrier = pltpu.get_barrier_semaphore()
+    for offset in offsets:
+        pl.semaphore_signal(
+            barrier,
+            inc=1,
+            device_id=(dp, lax.rem(me + offset, kv_count), tp),
+            device_id_type=MESH,
+        )
+    pl.semaphore_signal(barrier, inc=1, device_id=(dp, me, 1 - tp), device_id_type=MESH)
+
+    started = []
+
+    def send(kind, offset, source, target):
+        copy = pltpu.make_async_remote_copy(
+            src_ref=source,
+            dst_ref=target,
+            send_sem=send_sem.at[kind, offset],
+            recv_sem=recv_sem.at[kind, offset],
+            device_id=(dp, lax.rem(me + offset, kv_count), tp),
+            device_id_type=MESH,
+        )
+        copy.start()
+        started.append(copy)
+        return copy
+
+    loaded(tokens_ref, gain_ref)
+    flat = jnp.concatenate([tokens_ref[s].astype(jnp.float32) for s in range(seq_count)], 0)
+    inverse = lax.rsqrt(jnp.mean(flat * flat, axis=1, keepdims=True) + EPSILON)
+    start = pl.multiple_of(me * depth, depth)
+    own = jnp.concatenate(
+        [tokens_ref[s, :, pl.ds(start, depth)].astype(jnp.float32) for s in range(seq_count)], 0
+    )
+    own_gain = gain_ref[:, pl.ds(start, depth)].astype(jnp.float32)
+    normed = (own * inverse * own_gain).astype(jnp.bfloat16)
+    loaded(wq_ref)
+    q_part = dot_plain(normed, wq_ref[...])
+    for s in range(seq_count):
+        q_send[s] = q_part[s * prop : (s + 1) * prop]
+    pl.semaphore_wait(barrier, kv_count)
+    q_copies = [
+        send(0, offset, q_send.at[lax.rem(me + offset, kv_count)], q_recv.at[offset])
+        for offset in offsets
+    ]
+
+    loaded(wk_ref, wv_ref, wf_ref, gates_ref)
+    k_part = dot_plain(normed, wk_ref[...])
+    v_part = dot_plain(normed, wv_ref[...])
+    f_part = dot_plain(normed, wf_ref[...])
+    lane_pos = lax.broadcasted_iota(jnp.int32, (head_count, span), 1) + me * span
+    for s in range(seq_count):
+        rows = slice(s * prop, (s + 1) * prop)
+        kv_send[s, 0] = k_part[rows].astype(jnp.bfloat16)
+        kv_send[s, 1] = v_part[rows].astype(jnp.bfloat16)
+        valid = lengths_ref[s] + accepted_ref[s]
+        picked = jnp.where(lane_pos == valid - 1, gates_ref[s], 0.0)
+        last = jnp.sum(picked, axis=1, keepdims=True)
+        g_send[s, :prop, :] = jnp.zeros((prop, LANES), jnp.float32)
+        g_send[s, :prop, :head_count] = f_part[rows]
+        g_send[s, prop:, :] = jnp.broadcast_to(last, (head_count, LANES))
+
+    loaded(parents_ref)
+    parent_row = parents_ref[pl.ds(me, 1), :]
+    up = lax.broadcasted_iota(jnp.int32, (prop, prop), 0)
+    down = lax.broadcasted_iota(jnp.int32, (prop, prop), 1)
+    eye = (up == down).astype(jnp.bfloat16)
+    linked = jnp.where((up == parent_row) | (up == down), 1.0, 0.0)
+    for repeat in range(prop.bit_length()):
+        low = linked.astype(jnp.bfloat16)
+        linked = jnp.minimum(dot_plain(low, low), 1.0)
+    link = dot_rows(eye, linked.astype(jnp.bfloat16))
+
+    total = q_send[me]
+    for copy, offset in zip(q_copies, offsets):
+        copy.wait_recv()
+        total = total + q_recv[offset]
+    q_all[me] = total.astype(jnp.bfloat16)
+    qa_copies = {offset: send(1, offset, q_all.at[me], q_all.at[me]) for offset in offsets}
+    kv_copies = []
+    for offset in offsets:
+        there = lax.rem(me + offset, kv_count)
+        kv_copies.append(send(2, offset, kv_send.at[there], kv_recv.at[offset]))
+        kv_copies.append(send(3, offset, g_send.at[there], g_recv.at[offset]))
+
+    shape = (head_count, prop, width)
+    head_mask = (
+        lax.broadcasted_iota(jnp.int32, shape, 2) // head_size
+        == lax.broadcasted_iota(jnp.int32, shape, 0)
+    )
+    small = (head_count, prop, LANES)
+    small_lane = lax.broadcasted_iota(jnp.int32, small, 2)
+    small_head = lax.broadcasted_iota(jnp.int32, small, 0)
+
+    def spread(query):
+        wide = jnp.broadcast_to(query.astype(jnp.float32)[None], shape)
+        return jnp.where(head_mask, wide, 0.0).reshape(rows_all, width).astype(jnp.bfloat16)
+
+    def fold(wide):
+        return jnp.sum(jnp.where(head_mask, wide.reshape(shape), 0.0), axis=0)
+
+    def expand(column):
+        return fold(jnp.broadcast_to(column, (rows_all, width)))
+
+    def column_of(compact, first_lane):
+        wide = jnp.broadcast_to(compact[None], small)
+        taken = jnp.where(small_lane == small_head + first_lane, wide, 0.0)
+        return jnp.sum(taken.reshape(rows_all, LANES), axis=1, keepdims=True)
+
+    score_pos = lax.broadcasted_iota(jnp.int32, (rows_all, span), 1) + me * span
+
+    def attend(s):
+        valid = lengths_ref[s] + accepted_ref[s]
+        scores = dot_rows(spread(q_all[s]), keys_ref[s]) * scale
+        gates = jnp.broadcast_to(gates_ref[s][:, None, :], (head_count, prop, span))
+        scores = scores - gates.reshape(rows_all, span)
+        seen = score_pos < valid
+        highest = jnp.max(jnp.where(seen, scores, NEG_LARGE), axis=1, keepdims=True)
+        weights = jnp.where(seen, jnp.exp(scores - highest), 0.0)
+        normalizer = jnp.sum(weights, axis=1, keepdims=True)
+        w_send[s] = fold(dot_plain(weights.astype(jnp.bfloat16), values_ref[s])).astype(
+            jnp.bfloat16
+        )
+        both = jnp.where(
+            small_lane == small_head,
+            highest.reshape(head_count, prop, 1),
+            jnp.where(
+                small_lane == small_head + head_count,
+                normalizer.reshape(head_count, prop, 1),
+                0.0,
+            ),
+        )
+        st_send[s] = jnp.sum(both, axis=0)
+
+    loaded(keys_ref, values_ref)
+    attend(me)
+    w_copies = {}
+    for offset in offsets:
+        qa_copies[offset].wait_recv()
+        back = kv_count - offset
+        there = lax.rem(me + back, kv_count)
+        attend(there)
+        w_copies[back] = (
+            send(4, back, w_send.at[there], w_recv.at[back]),
+            send(5, back, st_send.at[there], st_recv.at[back]),
+        )
+
+    for copy in kv_copies:
+        copy.wait_recv()
+    fresh_k = kv_send[me, 0].astype(jnp.float32)
+    fresh_v = kv_send[me, 1].astype(jnp.float32)
+    gate_sum = g_send[me]
+    for offset in offsets:
+        fresh_k = fresh_k + kv_recv[offset, 0].astype(jnp.float32)
+        fresh_v = fresh_v + kv_recv[offset, 1].astype(jnp.float32)
+        gate_sum = gate_sum + g_recv[offset]
+    fresh_k = fresh_k.astype(jnp.bfloat16)
+    fresh_v = fresh_v.astype(jnp.bfloat16)
+    kv_all[me, 0] = fresh_k
+    kv_all[me, 1] = fresh_v
+    loaded(bias_ref)
+    gate_pre = gate_sum[:prop, :head_count] + bias_ref[...]
+    log_gate = -(jnp.maximum(-gate_pre, 0.0) + jnp.log1p(jnp.exp(-jnp.abs(gate_pre))))
+    climb = dot_plain(link, log_gate, HIGHEST)
+    chosen = (
+        lax.broadcasted_iota(jnp.int32, (head_count, head_count), 0)
+        == lax.broadcasted_iota(jnp.int32, (head_count, head_count), 1)
+    ).astype(jnp.float32)
+    climb_rows = dot_rows(chosen, climb, HIGHEST)
+    last_wide = gate_sum[prop:]
+    g_all[me] = jnp.zeros((head_count, LANES), jnp.float32)
+    g_all[me, :, :prop] = last_wide[:, :prop] + climb_rows
+
+    wide_climb = jnp.broadcast_to(climb[None], (head_count, prop, head_count))
+    climb_lane = lax.broadcasted_iota(jnp.int32, (head_count, prop, head_count), 2)
+    climb_head = lax.broadcasted_iota(jnp.int32, (head_count, prop, head_count), 0)
+    climb_col = jnp.sum(
+        jnp.where(climb_lane == climb_head, wide_climb, 0.0).reshape(rows_all, head_count),
+        axis=1,
+        keepdims=True,
+    )
+    near_shape = (head_count, prop, prop)
+    near = dot_rows(spread(q_all[me]), fresh_k) * scale + climb_col
+    near = near - jnp.broadcast_to(climb_rows[:, None, :], near_shape).reshape(rows_all, prop)
+    near_link = jnp.broadcast_to(link[None], near_shape).reshape(rows_all, prop) > 0.5
+    near_high = jnp.max(jnp.where(near_link, near, NEG_LARGE), axis=1, keepdims=True)
+    near_weights = jnp.where(near_link, jnp.exp(near - near_high), 0.0)
+    near_sum = jnp.sum(near_weights, axis=1, keepdims=True)
+    near_wide = dot_plain(near_weights.astype(jnp.bfloat16), fresh_v)
+    last_col = jnp.broadcast_to(
+        last_wide[:, None, :1], (head_count, prop, 1)
+    ).reshape(rows_all, 1)
+    shift = last_col + climb_col
+
+    loaded(head_gain_ref)
+    for pair in w_copies.values():
+        for copy in pair:
+            copy.wait_recv()
+    stats = [st_send[me]] + [st_recv[offset] for offset in offsets]
+    parts = [w_send[me]] + [w_recv[offset] for offset in offsets]
+    highs = [column_of(stat, 0) + shift for stat in stats]
+    sums = [column_of(stat, head_count) for stat in stats]
+    overall = near_high
+    for high in highs:
+        overall = jnp.maximum(overall, high)
+    near_factor = jnp.exp(near_high - overall)
+    factors = [jnp.exp(high - overall) for high in highs]
+    normalizer = near_sum * near_factor
+    for factor, part in zip(factors, sums):
+        normalizer = normalizer + factor * part
+    attended = fold(near_wide * (near_factor / normalizer))
+    for factor, part in zip(factors, parts):
+        attended = attended + expand(factor / normalizer) * part.astype(jnp.float32)
+    squares = jnp.where(head_mask, jnp.broadcast_to((attended * attended)[None], shape), 0.0)
+    square_col = jnp.sum(squares.reshape(rows_all, width), axis=1, keepdims=True)
+    rooted = lax.rsqrt(square_col * (1.0 / head_size) + EPSILON)
+    head_out = attended * expand(rooted) * head_gain_ref[...].astype(jnp.float32)
+    h_all[me] = head_out.astype(jnp.bfloat16)
+    h_copies = [send(6, offset, h_all.at[me], h_all.at[me]) for offset in offsets]
+    fresh_copies = []
+    for offset in offsets:
+        fresh_copies.append(send(7, offset, kv_all.at[me], kv_all.at[me]))
+        fresh_copies.append(send(8, offset, g_all.at[me], g_all.at[me]))
+
+    loaded(wo_ref)
+    for copy in h_copies:
+        copy.wait_recv()
+    heads = jnp.concatenate(
+        [h_all[s].astype(jnp.float32) for s in range(seq_count)], 0
+    ).astype(jnp.bfloat16)
+    there = pl.multiple_of((1 - tp) * half, half)
+    here = pl.multiple_of(tp * half, half)
+    o_send[...] = dot_plain(heads, wo_ref[:, pl.ds(there, half)])
+    pair = pltpu.make_async_remote_copy(
+        src_ref=o_send,
+        dst_ref=o_recv,
+        send_sem=pair_sem.at[0],
+        recv_sem=pair_sem.at[1],
+        device_id=(dp, me, 1 - tp),
+        device_id_type=MESH,
+    )
+    pair.start()
+    own_sum = dot_plain(heads, wo_ref[:, pl.ds(here, half)])
+    pair.wait()
+    own_sum = own_sum + o_recv[...]
+    for s in range(seq_count):
+        mixed_out[s] = own_sum[s * prop : (s + 1) * prop]
+    for copy in fresh_copies:
+        copy.wait_recv()
+    fresh_out[...] = kv_all[...]
+    fresh_gates_out[...] = g_all[...]
+    for copy in started:
+        copy.wait_send()
+
+
+def write_kernel(
+    lengths_ref,
+    accepted_ref,
+    mixed_ref,
+    fresh_ref,
+    fresh_gates_ref,
+    keys_ref,
+    values_ref,
+    gates_ref,
+    mixed_out,
+    keys_out,
+    values_out,
+    gates_out,
+):
+    seq = pl.program_id(0)
+    span = keys_ref.shape[1]
+    prop = fresh_ref.shape[2]
+    head_count = gates_ref.shape[1]
+    valid = lengths_ref[seq] + accepted_ref[seq]
+    first = lax.axis_index("kv") * span - valid
+    mixed_out[...] = mixed_ref[...]
+    down = lax.broadcasted_iota(jnp.int32, (span, prop), 0) + first
+    placed = (down == lax.broadcasted_iota(jnp.int32, (span, prop), 1)).astype(jnp.bfloat16)
+    row = lax.broadcasted_iota(jnp.int32, (span, keys_ref.shape[2]), 0) + first
+    landed = (row >= 0) & (row < prop)
+    for at, (source, target) in enumerate(((keys_ref, keys_out), (values_ref, values_out))):
+        written = dot_plain(placed, fresh_ref[0, at])
+        target[0] = jnp.where(landed, written, source[0].astype(jnp.float32)).astype(jnp.bfloat16)
+    over = lax.broadcasted_iota(jnp.int32, (prop, span), 1) + first
+    spot = (over == lax.broadcasted_iota(jnp.int32, (prop, span), 0)).astype(jnp.float32)
+    new_gates = dot_plain(fresh_gates_ref[0][:, :prop], spot, HIGHEST)
+    lane = lax.broadcasted_iota(jnp.int32, (head_count, span), 1) + first
+    gates_out[0] = jnp.where((lane >= 0) & (lane < prop), new_gates, gates_ref[0])
+
+
+def fused(
+    kv_count,
+    tokens,
+    norm_gain,
+    w_query,
+    w_key,
+    w_value,
+    w_forget,
+    forget_bias,
+    head_gain,
+    w_out,
+    cache_keys,
+    cache_values,
+    cache_gates,
+    lengths,
+    accepted,
+    parents,
+):
+    seq_count, prop, _ = tokens.shape
+    span, width = cache_keys.shape[1:]
+    head_count = cache_gates.shape[1]
+    half = w_out.shape[1] // 2
+    gain = norm_gain.reshape(1, -1)
+    bias = forget_bias.reshape(1, -1)
+    head_gain = head_gain.reshape(1, -1)
+    low, high = jnp.bfloat16, jnp.float32
+    large = (
+        tokens, gain, w_query, w_key, w_value, w_forget, bias, head_gain, w_out,
+        cache_keys, cache_values, cache_gates, parents,
+    )
+    vmem = pltpu.VMEM
+    scratch = [vmem(value.shape, value.dtype) for value in large]
+    block = (seq_count, prop, width)
+    pair = (seq_count, 2, prop, width)
+    scratch += [
+        vmem(block, high),
+        vmem(block, high),
+        vmem(block, low),
+        vmem(pair, low),
+        vmem(pair, low),
+        vmem(pair, low),
+        vmem((seq_count, prop + head_count, LANES), high),
+        vmem((seq_count, prop + head_count, LANES), high),
+        vmem((seq_count, head_count, LANES), high),
+        vmem(block, low),
+        vmem(block, low),
+        vmem((seq_count, prop, LANES), high),
+        vmem((seq_count, prop, LANES), high),
+        vmem(block, low),
+        vmem((seq_count * prop, half), high),
+        vmem((seq_count * prop, half), high),
+        pltpu.SemaphoreType.DMA((len(large),)),
+        pltpu.SemaphoreType.DMA((9, kv_count)),
+        pltpu.SemaphoreType.DMA((9, kv_count)),
+        pltpu.SemaphoreType.DMA((2,)),
+    ]
+    smem = pl.BlockSpec(memory_space=pltpu.SMEM)
+    mixed, fresh, fresh_gates = pl.pallas_call(
+        functools.partial(exchange_kernel, kv_count, head_count),
+        out_shape=(
+            jax.ShapeDtypeStruct((seq_count, prop, half), high),
+            jax.ShapeDtypeStruct(pair, low),
+            jax.ShapeDtypeStruct((seq_count, head_count, LANES), high),
+        ),
+        in_specs=[smem, smem] + [pl.BlockSpec(memory_space=pl.ANY)] * len(large),
+        out_specs=(pl.BlockSpec(memory_space=pltpu.VMEM),) * 3,
+        scratch_shapes=scratch,
+        compiler_params=pltpu.CompilerParams(
+            collective_id=0, has_side_effects=True, vmem_limit_bytes=32 * 1024 * 1024
+        ),
+        name="exchange",
+    )(lengths, accepted, *large)
+
+    def per_seq(*tail):
+        return pl.BlockSpec((1, *tail), lambda s: (s,) + (0,) * len(tail))
+
+    outs = (per_seq(prop, half), per_seq(span, width), per_seq(span, width), per_seq(head_count, span))
+    return pl.pallas_call(
+        write_kernel,
+        grid=(seq_count,),
+        out_shape=(
+            jax.ShapeDtypeStruct(mixed.shape, high),
+            jax.ShapeDtypeStruct(cache_keys.shape, low),
+            jax.ShapeDtypeStruct(cache_values.shape, low),
+            jax.ShapeDtypeStruct(cache_gates.shape, high),
+        ),
+        in_specs=[
+            smem,
+            smem,
+            outs[0],
+            per_seq(2, prop, width),
+            per_seq(head_count, LANES),
+            outs[1],
+            outs[2],
+            outs[3],
+        ],
+        out_specs=outs,
+        name="write",
+    )(lengths, accepted, mixed, fresh, fresh_gates, cache_keys, cache_values, cache_gates)
+
+
+def device_step(kv_count, tp_count, tokens, *rest):
+    seq_count, prop, _ = tokens.shape
+    head_count = rest[10].shape[1]
+    fits = seq_count == kv_count and tp_count == 2 and prop % 8 == 0 and prop <= LANES
+    if fits and kv_count > 1 and head_count % 8 == 0 and 2 * head_count <= LANES:
+        return fused(kv_count, tokens, *rest)
+    return local(tokens, *rest)
+
+
 def solution(mesh):
     placed = (
         P("dp", None, None),
@@ -192,7 +703,7 @@
         P("dp", None),
     )
     return jax.shard_map(
-        local,
+        functools.partial(device_step, mesh.shape["kv"], mesh.shape["tp"]),
         mesh=mesh,
         in_specs=placed,
         out_specs=(

time: 121 us -> 49.8 us (0.41)
  blocking collectives: 78.2 us -> 0 us
  Pallas kernels: 0 us -> 36.9 us
  between operations: 14.5 us -> 0.74 us
  matrix products: 10.9 us -> 0 us
  other arithmetic: 4.89 us -> 0 us
  waiting for transfers between devices: 2.2 us -> 0 us
  local copies, waits for them, and re-layouts: 10.1 us -> 11.6 us
    all_gather x3 -> x0, blocking collectives: 43.9 us -> none  [joined_2(): pieces = jax.tree.map(lambda part: lax.all_gather(part, axis), value)]
    pallas_call x0 -> x2, Pallas kernels: none -> 36.9 us  [the longest x1 32.6 us: fused(): pl.pallas_call(functools.partial(exchange_kernel, kv_count, head_count),...]
    psum x1 -> x0, blocking collectives: 34.3 us -> none  [local(): lax.psum((query_part, key_part, value_part, gate_part, last_part), 'kv')]
    dot_general x18 -> x0, matrix products: 10.9 us -> none  [the longest x5 1.77 us: ancestry(): jnp.einsum('bij,bjk->bik', linked, linked, precision=lax.Precision.HIGHEST)]
    unnamed x52 -> x35, local copies, waits for them, and re-layouts: 4.17 us -> 10.9 us
    add x8 -> x0, other arithmetic: 2.54 us -> none  [the longest x3 2.22 us: merge_pair(): first_part[1] * scale_first + second_part[1] * scale_second]
    reduce_scatter x1 -> x0, waiting for transfers between devices: 2.18 us -> none  [local(): lax.psum_scatter(partial_sum, 'tp', scatter_dimension=1, tiled=True)]
    mul x13 -> x0, local copies, waits for them, and re-layouts: 1.81 us -> none  [the longest x6 0.87 us: merge_pair(): first_part[2].reshape(seq_count, prop_count, head_count, -1)]
  transfers between devices with their start and end apart: 1 -> 0, of which waited for: 1 -> 0; matrix products, arithmetic and copies ran while one was open for 3% -> 0% of each run, Pallas kernels for 0% -> 0%
where the time goes in v1:
time: 49.8 us; the launch traced here: 49.2 us
  Pallas kernels  36.9 us (74%)
  local copies, waits for them, and re-layouts  11.6 us (23%)
  between operations  0.74 us (1%)
    pallas_call x1, Pallas kernels, fused(): pl.pallas_call(functools.partial(exchange_kernel, kv_count, head_count),...  32.6 us
    unnamed x35, local copies, waits for them, and re-layouts  10.9 us
    pallas_call x1, Pallas kernels, fused(): pl.pallas_call(write_kernel, grid=(seq_count,), out_shape=(jax.ShapeDtype...  4.28 us

profile of v1, /device:TPU:0, one launch (start us, length us, event | category | flops | bytes accessed | tf_op | source)
XLA Modules:
  0.0 49.2 jit_solution(16915581165474726029)
XLA Ops:
  0.7 0.7 %copy-done.16 = bf16[512]{0:T(512)(128)(2,1)S(1)} copy-done((bf16[512]{0:T(512)(128)(2,1)S(1)}, bf16[512]{0:T(512)(128)(2,1)}, u32[]{:S(2)}) %copy-start.16) | copy-done | bytes 1048
  1.3 0.7 %reshape.17.gain_hbm = bf16[1,2048]{1,0:T(2,128)(2,1)S(1)} reshape(bf16[2048]{0:T(1024)(128)(2,1)} %param.16) | data formatting | bytes 8192 | tf_op jit(solution)/shard_map/reshape | solution.py:599
  2.0 0.0 copy-start.8
  2.0 0.0 copy-start.11
  2.0 0.0 copy-start.12
  2.1 0.0 copy-start.13
  2.1 0.0 copy-start.14
  2.1 0.2 copy.19.wf_hbm
  2.2 0.5 %copy-done.8 = f32[4,8,256]{2,1,0:T(8,128)S(1)} copy-done((f32[4,8,256]{2,1,0:T(8,128)S(1)}, f32[4,8,256]{2,1,0:T(8,128)}, u32[]{:S(2)}) %copy-start.8) | copy-done | bytes 32792
  2.8 0.0 copy-done.11
  2.8 0.0 copy-done.13
  2.8 0.0 copy-start
  2.8 1.2 %copy-done = bf16[4,256,512]{2,1,0:T(8,128)(2,1)S(1)} copy-done((bf16[4,256,512]{2,1,0:T(8,128)(2,1)S(1)}, bf16[4,256,512]{2,1,0:T(8,128)(2,1)}, u32[]{:S(2)}) %copy-start) | copy-done | bytes 1048600
  4.0 1.2 %copy-done.1 = bf16[4,256,512]{2,1,0:T(8,128)(2,1)S(1)} copy-done((bf16[4,256,512]{2,1,0:T(8,128)(2,1)S(1)}, bf16[4,256,512]{2,1,0:T(8,128)(2,1)}, u32[]{:S(2)}) %copy-start.1) | copy-done | bytes 1048600
  5.2 1.0 %copy-done.2 = bf16[512,512]{1,0:T(8,128)(2,1)S(1)} copy-done((bf16[512,512]{1,0:T(8,128)(2,1)S(1)}, bf16[512,512]{1,0:T(8,128)(2,1)}, u32[]{:S(2)}) %copy-start.2) | copy-done | bytes 524312
  6.3 1.0 %copy-done.3 = bf16[512,512]{1,0:T(8,128)(2,1)S(1)} copy-done((bf16[512,512]{1,0:T(8,128)(2,1)S(1)}, bf16[512,512]{1,0:T(8,128)(2,1)}, u32[]{:S(2)}) %copy-start.3) | copy-done | bytes 524312
  7.3 1.0 %copy-done.4 = bf16[512,512]{1,0:T(8,128)(2,1)S(1)} copy-done((bf16[512,512]{1,0:T(8,128)(2,1)S(1)}, bf16[512,512]{1,0:T(8,128)(2,1)}, u32[]{:S(2)}) %copy-start.4) | copy-done | bytes 524312
  8.4 1.0 %copy-done.5 = bf16[512,512]{1,0:T(8,128)(2,1)S(1)} copy-done((bf16[512,512]{1,0:T(8,128)(2,1)S(1)}, bf16[512,512]{1,0:T(8,128)(2,1)}, u32[]{:S(2)}) %copy-start.5) | copy-done | bytes 524312
  9.4 1.0 %copy-done.6 = bf16[4,24,2048]{2,1,0:T(8,128)(2,1)S(1)} copy-done((bf16[4,24,2048]{2,1,0:T(8,128)(2,1)S(1)}, bf16[4,24,2048]{2,1,0:T(8,128)(2,1)}, u32[]{:S(2)}) %copy-start.6) | copy-done | bytes 393240
  10.4 32.6 %exchange.1 = (f32[4,24,256]{2,1,0:T(8,128)S(1)}, bf16[4,2,24,512]{3,2,1,0:T(8,128)(2,1)S(1)}, f32[4,8,128]{2,1,0:T(8,128)S(1)}) custom-call(s32[4]{0:T(128)S(1)} %copy-done.12, s32[4]{0:T(128)S(1)} %copy-done.13, bf16[4,24,2048]{2,1,0:T(8,128)(2,1)S(1)} %copy-done.6, bf16[1,2048]{1,0:T(2,128)(2,1)S(1)} %reshape.17.gain_hbm, bf16[512,512]{1,0:T(8,128)(2,1)S(1)} %copy-done.2, ...), custom_call_target="tpu_custom_call" | custom-call | tf_op jit(solution)/shard_map/exchange/pallas_call | solution.py:634
  43.0 0.7 %copy-done.7 = bf16[4,2,24,512]{3,2,1,0:T(8,128)(2,1)} copy-done((bf16[4,2,24,512]{3,2,1,0:T(8,128)(2,1)}, bf16[4,2,24,512]{3,2,1,0:T(8,128)(2,1)S(1)}, u32[]{:S(2)}) %copy-start.7) | copy-done | bytes 196632
  43.7 0.6 %copy-done.9 = f32[4,24,256]{2,1,0:T(8,128)} copy-done((f32[4,24,256]{2,1,0:T(8,128)}, f32[4,24,256]{2,1,0:T(8,128)S(1)}, u32[]{:S(2)}) %copy-start.9) | copy-done | bytes 98328
  44.3 0.6 %copy-done.10 = f32[4,8,128]{2,1,0:T(8,128)} copy-done((f32[4,8,128]{2,1,0:T(8,128)}, f32[4,8,128]{2,1,0:T(8,128)S(1)}, u32[]{:S(2)}) %copy-start.10) | copy-done | bytes 16408
  44.9 4.3 %write.1 = (f32[4,24,256]{2,1,0:T(8,128)}, bf16[4,256,512]{2,1,0:T(8,128)(2,1)}, bf16[4,256,512]{2,1,0:T(8,128)(2,1)}, f32[4,8,256]{2,1,0:T(8,128)}) custom-call(s32[4]{0:T(128)} %lengths_ref.3, s32[4]{0:T(128)} %accepted_ref.3, f32[4,24,256]{2,1,0:T(8,128)} %copy-done.9, bf16[4,2,24,512]{3,2,1,0:T(8,128)(2,1)} %copy-done.7, f32[4,8,128]{2,1,0:T(8,128)} %copy-done.10, ...), custom_call_target="tpu_custom_call" | custom-call | tf_op jit(solution)/shard_map/write/pallas_call | solution.py:654
  (15 shorter events, 0.0 us)
Async XLA Ops:
  0.6 0.7 %copy-start.16 = (bf16[512]{0:T(512)(128)(2,1)S(1)}, bf16[512]{0:T(512)(128)(2,1)}, u32[]{:S(2)}) copy-start(bf16[512]{0:T(512)(128)(2,1)} %param.22) | copy-start | bytes 3076
  0.6 1.4 %copy-start.15 = (bf16[512,8]{0,1:T(8,128)(2,1)S(1)}, bf16[512,8]{0,1:T(8,128)(2,1)}, u32[]{:S(2)}) copy-start(bf16[512,8]{0,1:T(8,128)(2,1)} %param.20) | copy-start | bytes 24580
  2.0 0.8 %copy-start.8 = (f32[4,8,256]{2,1,0:T(8,128)S(1)}, f32[4,8,256]{2,1,0:T(8,128)}, u32[]{:S(2)}) copy-start(f32[4,8,256]{2,1,0:T(8,128)} %gates_ref.1) | copy-start | bytes 98308
  2.0 0.8 %copy-start.11 = (s32[4,24]{1,0:T(4,128)S(1)}, s32[4,24]{1,0:T(4,128)}, u32[]{:S(2)}) copy-start(s32[4,24]{1,0:T(4,128)} %parents_hbm.1) | copy-start | bytes 1156
  2.0 0.7 %copy-start.12 = (s32[4]{0:T(128)S(1)}, s32[4]{0:T(128)}, u32[]{:S(2)}) copy-start(s32[4]{0:T(128)} %lengths_ref.3) | copy-start | bytes 52
  2.1 0.7 %copy-start.13 = (s32[4]{0:T(128)S(1)}, s32[4]{0:T(128)}, u32[]{:S(2)}) copy-start(s32[4]{0:T(128)} %accepted_ref.3) | copy-start | bytes 52
  2.1 0.7 %copy-start.14 = (f32[8]{0:T(128)S(1)}, f32[8]{0:T(128)}, u32[]{:S(2)}) copy-start(f32[8]{0:T(128)} %param.21) | copy-start | bytes 100
  2.8 1.2 %copy-start = (bf16[4,256,512]{2,1,0:T(8,128)(2,1)S(1)}, bf16[4,256,512]{2,1,0:T(8,128)(2,1)}, u32[]{:S(2)}) copy-start(bf16[4,256,512]{2,1,0:T(8,128)(2,1)} %keys_ref.1) | copy-start | bytes 3145732
  4.0 1.2 %copy-start.1 = (bf16[4,256,512]{2,1,0:T(8,128)(2,1)S(1)}, bf16[4,256,512]{2,1,0:T(8,128)(2,1)}, u32[]{:S(2)}) copy-start(bf16[4,256,512]{2,1,0:T(8,128)(2,1)} %values_ref.1) | copy-start | bytes 3145732
  5.2 1.0 %copy-start.2 = (bf16[512,512]{1,0:T(8,128)(2,1)S(1)}, bf16[512,512]{1,0:T(8,128)(2,1)}, u32[]{:S(2)}) copy-start(bf16[512,512]{1,0:T(8,128)(2,1)} %wq_hbm.1) | copy-start | bytes 1572868
  6.3 1.0 %copy-start.3 = (bf16[512,512]{1,0:T(8,128)(2,1)S(1)}, bf16[512,512]{1,0:T(8,128)(2,1)}, u32[]{:S(2)}) copy-start(bf16[512,512]{1,0:T(8,128)(2,1)} %wk_hbm.1) | copy-start | bytes 1572868
  7.3 1.0 %copy-start.4 = (bf16[512,512]{1,0:T(8,128)(2,1)S(1)}, bf16[512,512]{1,0:T(8,128)(2,1)}, u32[]{:S(2)}) copy-start(bf16[512,512]{1,0:T(8,128)(2,1)} %wv_hbm.1) | copy-start | bytes 1572868
  8.4 1.0 %copy-start.5 = (bf16[512,512]{1,0:T(8,128)(2,1)S(1)}, bf16[512,512]{1,0:T(8,128)(2,1)}, u32[]{:S(2)}) copy-start(bf16[512,512]{1,0:T(8,128)(2,1)} %wo_hbm.1) | copy-start | bytes 1572868
  9.4 1.0 %copy-start.6 = (bf16[4,24,2048]{2,1,0:T(8,128)(2,1)S(1)}, bf16[4,24,2048]{2,1,0:T(8,128)(2,1)}, u32[]{:S(2)}) copy-start(bf16[4,24,2048]{2,1,0:T(8,128)(2,1)} %tokens_hbm.1) | copy-start | bytes 1179652
  43.0 0.7 %copy-start.7 = (bf16[4,2,24,512]{3,2,1,0:T(8,128)(2,1)}, bf16[4,2,24,512]{3,2,1,0:T(8,128)(2,1)S(1)}, u32[]{:S(2)}) copy-start(bf16[4,2,24,512]{3,2,1,0:T(8,128)(2,1)S(1)} %get-tuple-element.8.fresh_ref) | copy-start | bytes 589828
  43.7 0.6 %copy-start.9 = (f32[4,24,256]{2,1,0:T(8,128)}, f32[4,24,256]{2,1,0:T(8,128)S(1)}, u32[]{:S(2)}) copy-start(f32[4,24,256]{2,1,0:T(8,128)S(1)} %get-tuple-element.7.mixed_ref) | copy-start | bytes 294916
  44.3 0.6 %copy-start.10 = (f32[4,8,128]{2,1,0:T(8,128)}, f32[4,8,128]{2,1,0:T(8,128)S(1)}, u32[]{:S(2)}) copy-start(f32[4,8,128]{2,1,0:T(8,128)S(1)} %get-tuple-element.9.fresh_gates_ref) | copy-start | bytes 49156

commit v2 on v1

--- a/solution.py
+++ b/solution.py
@@ -180,6 +180,8 @@
 HIGHEST = lax.Precision.HIGHEST
 MESH = pl.DeviceIdType.MESH
 LANES = 128
+WINDOW = 16
+VMEM_ALL = 67043328
 
 
 def dot_rows(left, right, precision=None):
@@ -246,6 +248,7 @@
     h_all,
     o_send,
     o_recv,
+    gain_wide,
     load_sem,
     send_sem,
     recv_sem,
@@ -318,7 +321,11 @@
     own = jnp.concatenate(
         [tokens_ref[s, :, pl.ds(start, depth)].astype(jnp.float32) for s in range(seq_count)], 0
     )
-    own_gain = gain_ref[:, pl.ds(start, depth)].astype(jnp.float32)
+    gain_wide[...] = gain_ref[...].astype(jnp.float32)
+    gain_rows = depth // LANES
+    own_gain = jnp.concatenate(
+        [gain_wide[pl.ds(me * gain_rows + at, 1), :] for at in range(gain_rows)], 1
+    )
     normed = (own * inverse * own_gain).astype(jnp.bfloat16)
     loaded(wq_ref)
     q_part = dot_plain(normed, wq_ref[...])
@@ -333,7 +340,7 @@
     loaded(wk_ref, wv_ref, wf_ref, gates_ref)
     k_part = dot_plain(normed, wk_ref[...])
     v_part = dot_plain(normed, wv_ref[...])
-    f_part = dot_plain(normed, wf_ref[...])
+    f_part = dot_rows(wf_ref[...], normed)
     lane_pos = lax.broadcasted_iota(jnp.int32, (head_count, span), 1) + me * span
     for s in range(seq_count):
         rows = slice(s * prop, (s + 1) * prop)
@@ -342,9 +349,8 @@
         valid = lengths_ref[s] + accepted_ref[s]
         picked = jnp.where(lane_pos == valid - 1, gates_ref[s], 0.0)
         last = jnp.sum(picked, axis=1, keepdims=True)
-        g_send[s, :prop, :] = jnp.zeros((prop, LANES), jnp.float32)
-        g_send[s, :prop, :head_count] = f_part[rows]
-        g_send[s, prop:, :] = jnp.broadcast_to(last, (head_count, LANES))
+        g_send[s] = jnp.broadcast_to(last, (head_count, LANES))
+        g_send[s, :, :prop] = f_part[:, rows]
 
     loaded(parents_ref)
     parent_row = parents_ref[pl.ds(me, 1), :]
@@ -376,7 +382,7 @@
     )
     small = (head_count, prop, LANES)
     small_lane = lax.broadcasted_iota(jnp.int32, small, 2)
-    small_head = lax.broadcasted_iota(jnp.int32, small, 0)
+    small_prop = lax.broadcasted_iota(jnp.int32, small, 1)
 
     def spread(query):
         wide = jnp.broadcast_to(query.astype(jnp.float32)[None], shape)
@@ -389,8 +395,8 @@
         return fold(jnp.broadcast_to(column, (rows_all, width)))
 
     def column_of(compact, first_lane):
-        wide = jnp.broadcast_to(compact[None], small)
-        taken = jnp.where(small_lane == small_head + first_lane, wide, 0.0)
+        wide = jnp.broadcast_to(compact[:, None, :], small)
+        taken = jnp.where(small_lane == small_prop + first_lane, wide, 0.0)
         return jnp.sum(taken.reshape(rows_all, LANES), axis=1, keepdims=True)
 
     score_pos = lax.broadcasted_iota(jnp.int32, (rows_all, span), 1) + me * span
@@ -408,15 +414,15 @@
             jnp.bfloat16
         )
         both = jnp.where(
-            small_lane == small_head,
+            small_lane == small_prop,
             highest.reshape(head_count, prop, 1),
             jnp.where(
-                small_lane == small_head + head_count,
+                small_lane == small_prop + prop,
                 normalizer.reshape(head_count, prop, 1),
                 0.0,
             ),
         )
-        st_send[s] = jnp.sum(both, axis=0)
+        st_send[s] = jnp.sum(both, axis=1)
 
     loaded(keys_ref, values_ref)
     attend(me)
@@ -445,47 +451,46 @@
     kv_all[me, 0] = fresh_k
     kv_all[me, 1] = fresh_v
     loaded(bias_ref)
-    gate_pre = gate_sum[:prop, :head_count] + bias_ref[...]
+    square = (head_count, head_count)
+    on_diagonal = lax.broadcasted_iota(jnp.int32, square, 0) == lax.broadcasted_iota(
+        jnp.int32, square, 1
+    )
+    bias = jnp.sum(
+        jnp.where(on_diagonal, jnp.broadcast_to(bias_ref[...], square), 0.0), axis=1, keepdims=True
+    )
+    gate_pre = gate_sum[:, :prop] + bias
     log_gate = -(jnp.maximum(-gate_pre, 0.0) + jnp.log1p(jnp.exp(-jnp.abs(gate_pre))))
-    climb = dot_plain(link, log_gate, HIGHEST)
-    chosen = (
-        lax.broadcasted_iota(jnp.int32, (head_count, head_count), 0)
-        == lax.broadcasted_iota(jnp.int32, (head_count, head_count), 1)
-    ).astype(jnp.float32)
-    climb_rows = dot_rows(chosen, climb, HIGHEST)
-    last_wide = gate_sum[prop:]
+    climb_rows = dot_plain(log_gate, linked, HIGHEST)
     g_all[me] = jnp.zeros((head_count, LANES), jnp.float32)
-    g_all[me, :, :prop] = last_wide[:, :prop] + climb_rows
-
-    wide_climb = jnp.broadcast_to(climb[None], (head_count, prop, head_count))
-    climb_lane = lax.broadcasted_iota(jnp.int32, (head_count, prop, head_count), 2)
-    climb_head = lax.broadcasted_iota(jnp.int32, (head_count, prop, head_count), 0)
+    g_all[me, :, :prop] = gate_sum[:, prop : prop + 1] + climb_rows
+    climb_wide = jnp.broadcast_to(climb_rows[:, None, :], (head_count, prop, prop))
     climb_col = jnp.sum(
-        jnp.where(climb_lane == climb_head, wide_climb, 0.0).reshape(rows_all, head_count),
+        jnp.where((up == down)[None], climb_wide, 0.0).reshape(rows_all, prop),
         axis=1,
         keepdims=True,
     )
     near_shape = (head_count, prop, prop)
     near = dot_rows(spread(q_all[me]), fresh_k) * scale + climb_col
-    near = near - jnp.broadcast_to(climb_rows[:, None, :], near_shape).reshape(rows_all, prop)
+    near = near - climb_wide.reshape(rows_all, prop)
     near_link = jnp.broadcast_to(link[None], near_shape).reshape(rows_all, prop) > 0.5
     near_high = jnp.max(jnp.where(near_link, near, NEG_LARGE), axis=1, keepdims=True)
     near_weights = jnp.where(near_link, jnp.exp(near - near_high), 0.0)
     near_sum = jnp.sum(near_weights, axis=1, keepdims=True)
     near_wide = dot_plain(near_weights.astype(jnp.bfloat16), fresh_v)
     last_col = jnp.broadcast_to(
-        last_wide[:, None, :1], (head_count, prop, 1)
+        gate_sum[:, prop : prop + 1][:, None, :], (head_count, prop, 1)
     ).reshape(rows_all, 1)
     shift = last_col + climb_col
 
     loaded(head_gain_ref)
+    head_gain = head_gain_ref[...].astype(jnp.float32)
     for pair in w_copies.values():
         for copy in pair:
             copy.wait_recv()
     stats = [st_send[me]] + [st_recv[offset] for offset in offsets]
     parts = [w_send[me]] + [w_recv[offset] for offset in offsets]
     highs = [column_of(stat, 0) + shift for stat in stats]
-    sums = [column_of(stat, head_count) for stat in stats]
+    sums = [column_of(stat, prop) for stat in stats]
     overall = near_high
     for high in highs:
         overall = jnp.maximum(overall, high)
@@ -500,7 +505,9 @@
     squares = jnp.where(head_mask, jnp.broadcast_to((attended * attended)[None], shape), 0.0)
     square_col = jnp.sum(squares.reshape(rows_all, width), axis=1, keepdims=True)
     rooted = lax.rsqrt(square_col * (1.0 / head_size) + EPSILON)
-    head_out = attended * expand(rooted) * head_gain_ref[...].astype(jnp.float32)
+    head_out = attended * expand(rooted) * jnp.concatenate(
+        [head_gain[at : at + 1] for at in range(width // LANES)], 1
+    )
     h_all[me] = head_out.astype(jnp.bfloat16)
     h_copies = [send(6, offset, h_all.at[me], h_all.at[me]) for offset in offsets]
     fresh_copies = []
@@ -545,33 +552,63 @@
     mixed_ref,
     fresh_ref,
     fresh_gates_ref,
-    keys_ref,
-    values_ref,
-    gates_ref,
+    keys_hbm,
+    values_hbm,
+    gates_hbm,
     mixed_out,
     keys_out,
     values_out,
     gates_out,
+    keys_ref,
+    values_ref,
+    gates_ref,
+    read_sem,
+    write_sem,
 ):
-    seq = pl.program_id(0)
-    span = keys_ref.shape[1]
+    seq_count, span, _ = keys_ref.shape
     prop = fresh_ref.shape[2]
     head_count = gates_ref.shape[1]
-    valid = lengths_ref[seq] + accepted_ref[seq]
-    first = lax.axis_index("kv") * span - valid
-    mixed_out[...] = mixed_ref[...]
-    down = lax.broadcasted_iota(jnp.int32, (span, prop), 0) + first
-    placed = (down == lax.broadcasted_iota(jnp.int32, (span, prop), 1)).astype(jnp.bfloat16)
-    row = lax.broadcasted_iota(jnp.int32, (span, keys_ref.shape[2]), 0) + first
-    landed = (row >= 0) & (row < prop)
-    for at, (source, target) in enumerate(((keys_ref, keys_out), (values_ref, values_out))):
-        written = dot_plain(placed, fresh_ref[0, at])
-        target[0] = jnp.where(landed, written, source[0].astype(jnp.float32)).astype(jnp.bfloat16)
-    over = lax.broadcasted_iota(jnp.int32, (prop, span), 1) + first
-    spot = (over == lax.broadcasted_iota(jnp.int32, (prop, span), 0)).astype(jnp.float32)
-    new_gates = dot_plain(fresh_gates_ref[0][:, :prop], spot, HIGHEST)
-    lane = lax.broadcasted_iota(jnp.int32, (head_count, span), 1) + first
-    gates_out[0] = jnp.where((lane >= 0) & (lane < prop), new_gates, gates_ref[0])
+    rows = -(-(prop + WINDOW - 1) // WINDOW) * WINDOW
+    reads = []
+    for s in range(seq_count):
+        triple = (
+            pltpu.make_async_copy(keys_hbm.at[s], keys_ref.at[s], read_sem.at[0, s]),
+            pltpu.make_async_copy(values_hbm.at[s], values_ref.at[s], read_sem.at[1, s]),
+            pltpu.make_async_copy(gates_hbm.at[s], gates_ref.at[s], read_sem.at[2, s]),
+        )
+        for copy in triple:
+            copy.start()
+        reads.append(triple)
+    writes = [pltpu.make_async_copy(mixed_ref, mixed_out, write_sem.at[3, 0])]
+    writes[0].start()
+    for s in range(seq_count):
+        valid = lengths_ref[s] + accepted_ref[s]
+        first = valid - lax.axis_index("kv") * span
+        window = jnp.clip(first // WINDOW * WINDOW, 0, span - rows)
+        window = pl.multiple_of(window, WINDOW)
+        down = lax.broadcasted_iota(jnp.int32, (rows, prop), 0) + (window - first)
+        placed = (down == lax.broadcasted_iota(jnp.int32, (rows, prop), 1)).astype(jnp.bfloat16)
+        row = lax.broadcasted_iota(jnp.int32, (rows, keys_ref.shape[2]), 0) + (window - first)
+        landed = (row >= 0) & (row < prop)
+        over = lax.broadcasted_iota(jnp.int32, (prop, span), 1) - first
+        spot = (over == lax.broadcasted_iota(jnp.int32, (prop, span), 0)).astype(jnp.float32)
+        new_gates = dot_plain(fresh_gates_ref[s][:, :prop], spot, HIGHEST)
+        lane = lax.broadcasted_iota(jnp.int32, (head_count, span), 1) - first
+        for at, (target, out) in enumerate(((keys_ref, keys_out), (values_ref, values_out))):
+            written = dot_plain(placed, fresh_ref[s, at])
+            reads[s][at].wait()
+            old = target[s, pl.ds(window, rows), :].astype(jnp.float32)
+            target[s, pl.ds(window, rows), :] = jnp.where(landed, written, old).astype(
+                jnp.bfloat16
+            )
+            writes.append(pltpu.make_async_copy(target.at[s], out.at[s], write_sem.at[at, s]))
+            writes[-1].start()
+        reads[s][2].wait()
+        gates_ref[s] = jnp.where((lane >= 0) & (lane < prop), new_gates, gates_ref[s])
+        writes.append(pltpu.make_async_copy(gates_ref.at[s], gates_out.at[s], write_sem.at[2, s]))
+        writes[-1].start()
+    for copy in writes:
+        copy.wait()
 
 
 def fused(
@@ -596,9 +633,10 @@
     span, width = cache_keys.shape[1:]
     head_count = cache_gates.shape[1]
     half = w_out.shape[1] // 2
-    gain = norm_gain.reshape(1, -1)
+    gain = norm_gain.reshape(-1, LANES)
+    w_forget = w_forget.T
     bias = forget_bias.reshape(1, -1)
-    head_gain = head_gain.reshape(1, -1)
+    head_gain = head_gain.reshape(-1, LANES)
     low, high = jnp.bfloat16, jnp.float32
     large = (
         tokens, gain, w_query, w_key, w_value, w_forget, bias, head_gain, w_out,
@@ -615,71 +653,75 @@
         vmem(pair, low),
         vmem(pair, low),
         vmem(pair, low),
-        vmem((seq_count, prop + head_count, LANES), high),
-        vmem((seq_count, prop + head_count, LANES), high),
+        vmem((seq_count, head_count, LANES), high),
+        vmem((seq_count, head_count, LANES), high),
         vmem((seq_count, head_count, LANES), high),
         vmem(block, low),
         vmem(block, low),
-        vmem((seq_count, prop, LANES), high),
-        vmem((seq_count, prop, LANES), high),
+        vmem((seq_count, head_count, LANES), high),
+        vmem((seq_count, head_count, LANES), high),
         vmem(block, low),
         vmem((seq_count * prop, half), high),
         vmem((seq_count * prop, half), high),
+        vmem(gain.shape, high),
         pltpu.SemaphoreType.DMA((len(large),)),
         pltpu.SemaphoreType.DMA((9, kv_count)),
         pltpu.SemaphoreType.DMA((9, kv_count)),
         pltpu.SemaphoreType.DMA((2,)),
     ]
+    kept = seq_count * (prop * half * 4 + 2 * prop * width * 2 + head_count * LANES * 4)
     smem = pl.BlockSpec(memory_space=pltpu.SMEM)
     mixed, fresh, fresh_gates = pl.pallas_call(
         functools.partial(exchange_kernel, kv_count, head_count),
         out_shape=(
-            jax.ShapeDtypeStruct((seq_count, prop, half), high),
-            jax.ShapeDtypeStruct(pair, low),
-            jax.ShapeDtypeStruct((seq_count, head_count, LANES), high),
+            pltpu.VMEM((seq_count, prop, half), high),
+            pltpu.VMEM(pair, low),
+            pltpu.VMEM((seq_count, head_count, LANES), high),
         ),
-        in_specs=[smem, smem] + [pl.BlockSpec(memory_space=pl.ANY)] * len(large),
+        in_specs=[smem, smem] + [pl.BlockSpec(memory_space=pltpu.HBM)] * len(large),
         out_specs=(pl.BlockSpec(memory_space=pltpu.VMEM),) * 3,
         scratch_shapes=scratch,
         compiler_params=pltpu.CompilerParams(
-            collective_id=0, has_side_effects=True, vmem_limit_bytes=32 * 1024 * 1024
+            collective_id=0, has_side_effects=True, vmem_limit_bytes=VMEM_ALL - kept
         ),
         name="exchange",
     )(lengths, accepted, *large)
 
-    def per_seq(*tail):
-        return pl.BlockSpec((1, *tail), lambda s: (s,) + (0,) * len(tail))
-
-    outs = (per_seq(prop, half), per_seq(span, width), per_seq(span, width), per_seq(head_count, span))
+    held = pl.BlockSpec(memory_space=pltpu.VMEM)
+    far = pl.BlockSpec(memory_space=pltpu.HBM)
     return pl.pallas_call(
         write_kernel,
-        grid=(seq_count,),
         out_shape=(
             jax.ShapeDtypeStruct(mixed.shape, high),
             jax.ShapeDtypeStruct(cache_keys.shape, low),
             jax.ShapeDtypeStruct(cache_values.shape, low),
             jax.ShapeDtypeStruct(cache_gates.shape, high),
         ),
-        in_specs=[
-            smem,
-            smem,
-            outs[0],
-            per_seq(2, prop, width),
-            per_seq(head_count, LANES),
-            outs[1],
-            outs[2],
-            outs[3],
+        in_specs=[smem, smem, held, held, held, far, far, far],
+        out_specs=(far,) * 4,
+        scratch_shapes=[
+            vmem(cache_keys.shape, low),
+            vmem(cache_values.shape, low),
+            vmem(cache_gates.shape, high),
+            pltpu.SemaphoreType.DMA((3, seq_count)),
+            pltpu.SemaphoreType.DMA((4, seq_count)),
         ],
-        out_specs=outs,
+        compiler_params=pltpu.CompilerParams(vmem_limit_bytes=VMEM_ALL - kept),
         name="write",
     )(lengths, accepted, mixed, fresh, fresh_gates, cache_keys, cache_values, cache_gates)
+
+
+def span_fits(*rest):
+    depth, width = rest[1].shape
+    span = rest[8].shape[1]
+    return span % WINDOW == span % LANES == depth % LANES == width % LANES == 0
 
 
 def device_step(kv_count, tp_count, tokens, *rest):
     seq_count, prop, _ = tokens.shape
     head_count = rest[10].shape[1]
-    fits = seq_count == kv_count and tp_count == 2 and prop % 8 == 0 and prop <= LANES
-    if fits and kv_count > 1 and head_count % 8 == 0 and 2 * head_count <= LANES:
+    fits = seq_count == kv_count and tp_count == 2 and prop % 8 == 0 and 2 * prop <= LANES
+    if fits and kv_count > 1 and head_count % 8 == 0 and span_fits(*rest):
         return fused(kv_count, tokens, *rest)
     return local(tokens, *rest)
 

time: 49.8 us -> 35.7 us (0.72)
  local copies, waits for them, and re-layouts: 11.6 us -> 1.91 us
  Pallas kernels: 36.9 us -> 33 us
    unnamed x35 -> x6, local copies, waits for them, and re-layouts: 10.9 us -> 1.91 us
    pallas_call x1, Pallas kernels: 32.6 us -> 29 us  [fused(): pl.pallas_call(functools.partial(exchange_kernel, kv_count, head_count),...]
    reshape x2 -> x0, local copies, waits for them, and re-layouts: 0.7 us -> none  [the longest x1 0.69 us: fused(): gain = norm_gain.reshape(1, -1)]
where the time goes in v2:
time: 35.7 us; the launch traced here: 35.5 us
  Pallas kernels  33 us (92%)
  local copies, waits for them, and re-layouts  1.91 us (5%)
  between operations  0.65 us (2%)
    pallas_call x1, Pallas kernels, fused(): pl.pallas_call(functools.partial(exchange_kernel, kv_count, head_count),...  29 us
    pallas_call x1, Pallas kernels, fused(): pl.pallas_call(write_kernel, out_shape=(jax.ShapeDtypeStruct(mixed.shape,...  4.02 us
    unnamed x6, local copies, waits for them, and re-layouts  1.91 us

profile of v2, /device:TPU:0, one launch (start us, length us, event | category | flops | bytes accessed | tf_op | source)
XLA Modules:
  0.0 35.5 jit_solution(12634781821002600589)
XLA Ops:
  0.6 29.0 %exchange.1 = (f32[4,24,256]{2,1,0:T(8,128)S(1)}, bf16[4,2,24,512]{3,2,1,0:T(8,128)(2,1)S(1)}, f32[4,8,128]{2,1,0:T(8,128)S(1)}) custom-call(s32[4]{0:T(128)} %lengths_ref.3, s32[4]{0:T(128)} %accepted_ref.3, bf16[4,24,2048]{2,1,0:T(8,128)(2,1)} %tokens_hbm.1, bf16[16,128]{1,0:T(8,128)(2,1)} %bitcast.5, bf16[512,512]{1,0:T(8,128)(2,1)} %wq_hbm.1, ...), custom_call_target="tpu_custom_call" | custom-call | tf_op jit(solution)/shard_map/exchange/pallas_call | solution.py:674
  29.6 0.0 copy-start
  29.6 0.7 %copy-done = bf16[4,2,24,512]{3,2,1,0:T(8,128)(2,1)} copy-done((bf16[4,2,24,512]{3,2,1,0:T(8,128)(2,1)}, bf16[4,2,24,512]{3,2,1,0:T(8,128)(2,1)S(1)}, u32[]{:S(2)}) %copy-start) | copy-done | bytes 196632
  30.3 0.0 copy-start.1
  30.3 0.6 %copy-done.1 = f32[4,24,256]{2,1,0:T(8,128)} copy-done((f32[4,24,256]{2,1,0:T(8,128)}, f32[4,24,256]{2,1,0:T(8,128)S(1)}, u32[]{:S(2)}) %copy-start.1) | copy-done | bytes 98328
  30.9 0.0 copy-start.2
  30.9 0.6 %copy-done.2 = f32[4,8,128]{2,1,0:T(8,128)} copy-done((f32[4,8,128]{2,1,0:T(8,128)}, f32[4,8,128]{2,1,0:T(8,128)S(1)}, u32[]{:S(2)}) %copy-start.2) | copy-done | bytes 16408
  31.5 4.0 %write.1 = (f32[4,24,256]{2,1,0:T(8,128)}, bf16[4,256,512]{2,1,0:T(8,128)(2,1)}, bf16[4,256,512]{2,1,0:T(8,128)(2,1)}, f32[4,8,256]{2,1,0:T(8,128)}) custom-call(s32[4]{0:T(128)} %lengths_ref.3, s32[4]{0:T(128)} %accepted_ref.3, f32[4,24,256]{2,1,0:T(8,128)} %copy-done.1, bf16[4,2,24,512]{3,2,1,0:T(8,128)(2,1)} %copy-done, f32[4,8,128]{2,1,0:T(8,128)} %copy-done.2, ...), custom_call_target="tpu_custom_call" | custom-call | tf_op jit(solution)/shard_map/write/pallas_call | solution.py:692
Async XLA Ops:
  29.6 0.7 %copy-start = (bf16[4,2,24,512]{3,2,1,0:T(8,128)(2,1)}, bf16[4,2,24,512]{3,2,1,0:T(8,128)(2,1)S(1)}, u32[]{:S(2)}) copy-start(bf16[4,2,24,512]{3,2,1,0:T(8,128)(2,1)S(1)} %get-tuple-element.8.fresh_ref) | copy-start | bytes 589828
  30.3 0.6 %copy-start.1 = (f32[4,24,256]{2,1,0:T(8,128)}, f32[4,24,256]{2,1,0:T(8,128)S(1)}, u32[]{:S(2)}) copy-start(f32[4,24,256]{2,1,0:T(8,128)S(1)} %get-tuple-element.7.mixed_ref) | copy-start | bytes 294916
  30.9 0.6 %copy-start.2 = (f32[4,8,128]{2,1,0:T(8,128)}, f32[4,8,128]{2,1,0:T(8,128)S(1)}, u32[]{:S(2)}) copy-start(f32[4,8,128]{2,1,0:T(8,128)S(1)} %get-tuple-element.9.fresh_gates_ref) | copy-start | bytes 49156

commit v3 on v2

--- a/solution.py
+++ b/solution.py
@@ -219,6 +219,9 @@
     mixed_out,
     fresh_out,
     fresh_gates_out,
+    keys_ref,
+    values_ref,
+    gates_ref,
     tokens_ref,
     gain_ref,
     wq_ref,
@@ -228,9 +231,6 @@
     bias_ref,
     head_gain_ref,
     wo_ref,
-    keys_ref,
-    values_ref,
-    gates_ref,
     parents_ref,
     q_send,
     q_recv,
@@ -552,61 +552,63 @@
     mixed_ref,
     fresh_ref,
     fresh_gates_ref,
-    keys_hbm,
-    values_hbm,
-    gates_hbm,
+    keys_ref,
+    values_ref,
+    gates_ref,
     mixed_out,
     keys_out,
     values_out,
     gates_out,
-    keys_ref,
-    values_ref,
-    gates_ref,
-    read_sem,
+    window_ref,
+    new_gates_ref,
+    bulk_sem,
     write_sem,
 ):
-    seq_count, span, _ = keys_ref.shape
+    seq_count, span, width = keys_ref.shape
     prop = fresh_ref.shape[2]
     head_count = gates_ref.shape[1]
-    rows = -(-(prop + WINDOW - 1) // WINDOW) * WINDOW
-    reads = []
-    for s in range(seq_count):
-        triple = (
-            pltpu.make_async_copy(keys_hbm.at[s], keys_ref.at[s], read_sem.at[0, s]),
-            pltpu.make_async_copy(values_hbm.at[s], values_ref.at[s], read_sem.at[1, s]),
-            pltpu.make_async_copy(gates_hbm.at[s], gates_ref.at[s], read_sem.at[2, s]),
-        )
-        for copy in triple:
-            copy.start()
-        reads.append(triple)
-    writes = [pltpu.make_async_copy(mixed_ref, mixed_out, write_sem.at[3, 0])]
-    writes[0].start()
+    rows = window_ref.shape[2]
+    caches = ((keys_ref, keys_out), (values_ref, values_out))
+    bulk = [
+        pltpu.make_async_copy(source, out, bulk_sem.at[at])
+        for at, (source, out) in enumerate(caches + ((mixed_ref, mixed_out),))
+    ]
+    for copy in bulk:
+        copy.start()
+    starts = []
     for s in range(seq_count):
         valid = lengths_ref[s] + accepted_ref[s]
         first = valid - lax.axis_index("kv") * span
         window = jnp.clip(first // WINDOW * WINDOW, 0, span - rows)
         window = pl.multiple_of(window, WINDOW)
-        down = lax.broadcasted_iota(jnp.int32, (rows, prop), 0) + (window - first)
-        placed = (down == lax.broadcasted_iota(jnp.int32, (rows, prop), 1)).astype(jnp.bfloat16)
-        row = lax.broadcasted_iota(jnp.int32, (rows, keys_ref.shape[2]), 0) + (window - first)
-        landed = (row >= 0) & (row < prop)
+        starts.append(window)
         over = lax.broadcasted_iota(jnp.int32, (prop, span), 1) - first
         spot = (over == lax.broadcasted_iota(jnp.int32, (prop, span), 0)).astype(jnp.float32)
         new_gates = dot_plain(fresh_gates_ref[s][:, :prop], spot, HIGHEST)
         lane = lax.broadcasted_iota(jnp.int32, (head_count, span), 1) - first
-        for at, (target, out) in enumerate(((keys_ref, keys_out), (values_ref, values_out))):
+        new_gates_ref[s] = jnp.where((lane >= 0) & (lane < prop), new_gates, gates_ref[s])
+        down = lax.broadcasted_iota(jnp.int32, (rows, prop), 0) + (window - first)
+        placed = (down == lax.broadcasted_iota(jnp.int32, (rows, prop), 1)).astype(jnp.bfloat16)
+        row = lax.broadcasted_iota(jnp.int32, (rows, width), 0) + (window - first)
+        landed = (row >= 0) & (row < prop)
+        for at, (source, _) in enumerate(caches):
             written = dot_plain(placed, fresh_ref[s, at])
-            reads[s][at].wait()
-            old = target[s, pl.ds(window, rows), :].astype(jnp.float32)
-            target[s, pl.ds(window, rows), :] = jnp.where(landed, written, old).astype(
-                jnp.bfloat16
+            old = source[s, pl.ds(window, rows), :].astype(jnp.float32)
+            window_ref[at, s] = jnp.where(landed, written, old).astype(jnp.bfloat16)
+    writes = [pltpu.make_async_copy(new_gates_ref, gates_out, write_sem.at[2, 0])]
+    writes[0].start()
+    for at, (_, out) in enumerate(caches):
+        bulk[at].wait()
+        for s in range(seq_count):
+            writes.append(
+                pltpu.make_async_copy(
+                    window_ref.at[at, s],
+                    out.at[s, pl.ds(starts[s], rows), :],
+                    write_sem.at[at, s],
+                )
             )
-            writes.append(pltpu.make_async_copy(target.at[s], out.at[s], write_sem.at[at, s]))
             writes[-1].start()
-        reads[s][2].wait()
-        gates_ref[s] = jnp.where((lane >= 0) & (lane < prop), new_gates, gates_ref[s])
-        writes.append(pltpu.make_async_copy(gates_ref.at[s], gates_out.at[s], write_sem.at[2, s]))
-        writes[-1].start()
+    bulk[2].wait()
     for copy in writes:
         copy.wait()
 
@@ -643,7 +645,7 @@
         cache_keys, cache_values, cache_gates, parents,
     )
     vmem = pltpu.VMEM
-    scratch = [vmem(value.shape, value.dtype) for value in large]
+    scratch = [vmem(value.shape, value.dtype) for value in large[:9] + large[12:]]
     block = (seq_count, prop, width)
     pair = (seq_count, 2, prop, width)
     scratch += [
@@ -669,17 +671,24 @@
         pltpu.SemaphoreType.DMA((9, kv_count)),
         pltpu.SemaphoreType.DMA((2,)),
     ]
-    kept = seq_count * (prop * half * 4 + 2 * prop * width * 2 + head_count * LANES * 4)
+    kept = seq_count * (
+        prop * half * 4
+        + 2 * (prop + span) * width * 2
+        + head_count * (LANES + span) * 4
+    )
     smem = pl.BlockSpec(memory_space=pltpu.SMEM)
-    mixed, fresh, fresh_gates = pl.pallas_call(
+    held_parts = pl.pallas_call(
         functools.partial(exchange_kernel, kv_count, head_count),
         out_shape=(
             pltpu.VMEM((seq_count, prop, half), high),
             pltpu.VMEM(pair, low),
             pltpu.VMEM((seq_count, head_count, LANES), high),
+            pltpu.VMEM(cache_keys.shape, low),
+            pltpu.VMEM(cache_values.shape, low),
+            pltpu.VMEM(cache_gates.shape, high),
         ),
         in_specs=[smem, smem] + [pl.BlockSpec(memory_space=pltpu.HBM)] * len(large),
-        out_specs=(pl.BlockSpec(memory_space=pltpu.VMEM),) * 3,
+        out_specs=(pl.BlockSpec(memory_space=pltpu.VMEM),) * 6,
         scratch_shapes=scratch,
         compiler_params=pltpu.CompilerParams(
             collective_id=0, has_side_effects=True, vmem_limit_bytes=VMEM_ALL - kept
@@ -688,33 +697,33 @@
     )(lengths, accepted, *large)
 
     held = pl.BlockSpec(memory_space=pltpu.VMEM)
+    rows = -(-(prop + WINDOW - 1) // WINDOW) * WINDOW
     far = pl.BlockSpec(memory_space=pltpu.HBM)
     return pl.pallas_call(
         write_kernel,
         out_shape=(
-            jax.ShapeDtypeStruct(mixed.shape, high),
+            jax.ShapeDtypeStruct((seq_count, prop, half), high),
             jax.ShapeDtypeStruct(cache_keys.shape, low),
             jax.ShapeDtypeStruct(cache_values.shape, low),
             jax.ShapeDtypeStruct(cache_gates.shape, high),
         ),
-        in_specs=[smem, smem, held, held, held, far, far, far],
+        in_specs=[smem, smem] + [held] * 6,
         out_specs=(far,) * 4,
         scratch_shapes=[
-            vmem(cache_keys.shape, low),
-            vmem(cache_values.shape, low),
+            vmem((2, seq_count, rows, width), low),
             vmem(cache_gates.shape, high),
+            pltpu.SemaphoreType.DMA((3,)),
             pltpu.SemaphoreType.DMA((3, seq_count)),
-            pltpu.SemaphoreType.DMA((4, seq_count)),
         ],
-        compiler_params=pltpu.CompilerParams(vmem_limit_bytes=VMEM_ALL - kept),
+        compiler_params=pltpu.CompilerParams(vmem_limit_bytes=8 * 1024 * 1024),
         name="write",
-    )(lengths, accepted, mixed, fresh, fresh_gates, cache_keys, cache_values, cache_gates)
+    )(lengths, accepted, *held_parts)
 
 
 def span_fits(*rest):
     depth, width = rest[1].shape
     span = rest[8].shape[1]
-    return span % WINDOW == span % LANES == depth % LANES == width % LANES == 0
+    return span >= 4 * WINDOW and span % WINDOW == span % LANES == depth % LANES == width % LANES == 0
 
 
 def device_step(kv_count, tp_count, tokens, *rest):

time: 35.7 us -> 33.2 us (0.930)
  Pallas kernels: 33 us -> 31.7 us
  local copies, waits for them, and re-layouts: 1.91 us -> 0.66 us
    pallas_call x1, Pallas kernels: 4.02 us -> 2.68 us  [fused(): pl.pallas_call(write_kernel, out_shape=(jax.ShapeDtypeStruct((seq_count,...]
    unnamed x6 -> x4, local copies, waits for them, and re-layouts: 1.91 us -> 0.66 us
where the time goes in v3:
time: 33.2 us; the launch traced here: 33 us
  Pallas kernels  31.7 us (95%)
  local copies, waits for them, and re-layouts  0.66 us (2%)
  between operations  0.66 us (2%)
    pallas_call x1, Pallas kernels, fused(): pl.pallas_call(functools.partial(exchange_kernel, kv_count, head_count),...  29 us
    pallas_call x1, Pallas kernels, fused(): pl.pallas_call(write_kernel, out_shape=(jax.ShapeDtypeStruct((seq_count,...  2.68 us

profile of v3, /device:TPU:0, one launch (start us, length us, event | category | flops | bytes accessed | tf_op | source)
XLA Modules:
  0.0 33.0 jit_solution(14936722665808205465)
XLA Ops:
  0.6 29.0 %exchange.1 = (f32[4,24,256]{2,1,0:T(8,128)S(1)}, bf16[4,2,24,512]{3,2,1,0:T(8,128)(2,1)S(1)}, f32[4,8,128]{2,1,0:T(8,128)S(1)}, bf16[4,256,512]{2,1,0:T(8,128)(...) custom-call(s32[4]{0:T(128)} %lengths_ref.3, s32[4]{0:T(128)} %accepted_ref.3, ...), custom_call_target="tpu_custom_call" | custom-call | tf_op jit(solution)/shard_map/exchange/pallas_call | solution.py:680
  29.6 0.0 copy-start
  29.6 0.0 copy-start.1
  29.7 0.6 %copy-done = s32[4]{0:T(128)S(1)} copy-done((s32[4]{0:T(128)S(1)}, s32[4]{0:T(128)}, u32[]{:S(2)}) %copy-start) | copy-done | bytes 40
  30.3 0.0 copy-done.1
  30.3 2.7 %write.1 = (f32[4,24,256]{2,1,0:T(8,128)}, bf16[4,256,512]{2,1,0:T(8,128)(2,1)}, bf16[4,256,512]{2,1,0:T(8,128)(2,1)}, f32[4,8,256]{2,1,0:T(8,128)}) custom-call(s32[4]{0:T(128)S(1)} %copy-done, s32[4]{0:T(128)S(1)} %copy-done.1, f32[4,24,256]{2,1,0:T(8,128)S(1)} %get-tuple-element.10.mixed_ref, bf16[4,2,24,512]{3,2,1,0:T(8,128)(2,1)S(1)} %get-tuple-element.11.fresh_ref, ...), custom_call_target="tpu_custom_call" | custom-call | tf_op jit(solution)/shard_map/write/pallas_call | solution.py:702
Async XLA Ops:
  29.6 0.7 %copy-start = (s32[4]{0:T(128)S(1)}, s32[4]{0:T(128)}, u32[]{:S(2)}) copy-start(s32[4]{0:T(128)} %lengths_ref.3) | copy-start | bytes 52
  29.6 0.7 %copy-start.1 = (s32[4]{0:T(128)S(1)}, s32[4]{0:T(128)}, u32[]{:S(2)}) copy-start(s32[4]{0:T(128)} %accepted_ref.3) | copy-start | bytes 52

commit v4 on v3

--- a/solution.py
+++ b/solution.py
@@ -216,6 +216,7 @@
     values_hbm,
     gates_hbm,
     parents_hbm,
+    valid_out,
     mixed_out,
     fresh_out,
     fresh_gates_out,
@@ -339,12 +340,14 @@
 
     loaded(wk_ref, wv_ref, wf_ref, gates_ref)
     k_part = dot_plain(normed, wk_ref[...])
+    for s in range(seq_count):
+        kv_send[s, 0] = k_part[s * prop : (s + 1) * prop].astype(jnp.bfloat16)
     v_part = dot_plain(normed, wv_ref[...])
     f_part = dot_rows(wf_ref[...], normed)
     lane_pos = lax.broadcasted_iota(jnp.int32, (head_count, span), 1) + me * span
     for s in range(seq_count):
+        valid_out[s] = jnp.full((8, LANES), lengths_ref[s] + accepted_ref[s], jnp.int32)
         rows = slice(s * prop, (s + 1) * prop)
-        kv_send[s, 0] = k_part[rows].astype(jnp.bfloat16)
         kv_send[s, 1] = v_part[rows].astype(jnp.bfloat16)
         valid = lengths_ref[s] + accepted_ref[s]
         picked = jnp.where(lane_pos == valid - 1, gates_ref[s], 0.0)
@@ -372,7 +375,8 @@
     kv_copies = []
     for offset in offsets:
         there = lax.rem(me + offset, kv_count)
-        kv_copies.append(send(2, offset, kv_send.at[there], kv_recv.at[offset]))
+        kv_copies.append(send(2, offset, kv_send.at[there, 0], kv_recv.at[offset, 0]))
+        kv_copies.append(send(9, offset, kv_send.at[there, 1], kv_recv.at[offset, 1]))
         kv_copies.append(send(3, offset, g_send.at[there], g_recv.at[offset]))
 
     shape = (head_count, prop, width)
@@ -481,6 +485,8 @@
         gate_sum[:, prop : prop + 1][:, None, :], (head_count, prop, 1)
     ).reshape(rows_all, 1)
     shift = last_col + climb_col
+
+    fresh_copies = [send(7, offset, kv_all.at[me, 0], kv_all.at[me, 0]) for offset in offsets]
 
     loaded(head_gain_ref)
     head_gain = head_gain_ref[...].astype(jnp.float32)
@@ -510,9 +516,8 @@
     )
     h_all[me] = head_out.astype(jnp.bfloat16)
     h_copies = [send(6, offset, h_all.at[me], h_all.at[me]) for offset in offsets]
-    fresh_copies = []
     for offset in offsets:
-        fresh_copies.append(send(7, offset, kv_all.at[me], kv_all.at[me]))
+        fresh_copies.append(send(10, offset, kv_all.at[me, 1], kv_all.at[me, 1]))
         fresh_copies.append(send(8, offset, g_all.at[me], g_all.at[me]))
 
     loaded(wo_ref)
@@ -547,8 +552,7 @@
 
 
 def write_kernel(
-    lengths_ref,
-    accepted_ref,
+    valid_ref,
     mixed_ref,
     fresh_ref,
     fresh_gates_ref,
@@ -577,7 +581,7 @@
         copy.start()
     starts = []
     for s in range(seq_count):
-        valid = lengths_ref[s] + accepted_ref[s]
+        valid = jnp.max(valid_ref[s])
         first = valid - lax.axis_index("kv") * span
         window = jnp.clip(first // WINDOW * WINDOW, 0, span - rows)
         window = pl.multiple_of(window, WINDOW)
@@ -667,19 +671,21 @@
         vmem((seq_count * prop, half), high),
         vmem(gain.shape, high),
         pltpu.SemaphoreType.DMA((len(large),)),
-        pltpu.SemaphoreType.DMA((9, kv_count)),
-        pltpu.SemaphoreType.DMA((9, kv_count)),
+        pltpu.SemaphoreType.DMA((11, kv_count)),
+        pltpu.SemaphoreType.DMA((11, kv_count)),
         pltpu.SemaphoreType.DMA((2,)),
     ]
     kept = seq_count * (
         prop * half * 4
         + 2 * (prop + span) * width * 2
         + head_count * (LANES + span) * 4
+        + 8 * LANES * 4
     )
     smem = pl.BlockSpec(memory_space=pltpu.SMEM)
     held_parts = pl.pallas_call(
         functools.partial(exchange_kernel, kv_count, head_count),
         out_shape=(
+            pltpu.VMEM((seq_count, 8, LANES), jnp.int32),
             pltpu.VMEM((seq_count, prop, half), high),
             pltpu.VMEM(pair, low),
             pltpu.VMEM((seq_count, head_count, LANES), high),
@@ -688,7 +694,7 @@
             pltpu.VMEM(cache_gates.shape, high),
         ),
         in_specs=[smem, smem] + [pl.BlockSpec(memory_space=pltpu.HBM)] * len(large),
-        out_specs=(pl.BlockSpec(memory_space=pltpu.VMEM),) * 6,
+        out_specs=(pl.BlockSpec(memory_space=pltpu.VMEM),) * 7,
         scratch_shapes=scratch,
         compiler_params=pltpu.CompilerParams(
             collective_id=0, has_side_effects=True, vmem_limit_bytes=VMEM_ALL - kept
@@ -707,7 +713,7 @@
             jax.ShapeDtypeStruct(cache_values.shape, low),
             jax.ShapeDtypeStruct(cache_gates.shape, high),
         ),
-        in_specs=[smem, smem] + [held] * 6,
+        in_specs=[held] * 7,
         out_specs=(far,) * 4,
         scratch_shapes=[
             vmem((2, seq_count, rows, width), low),
@@ -717,7 +723,7 @@
         ],
         compiler_params=pltpu.CompilerParams(vmem_limit_bytes=8 * 1024 * 1024),
         name="write",
-    )(lengths, accepted, *held_parts)
+    )(*held_parts)
 
 
 def span_fits(*rest):

time: 33.2 us -> 31.3 us (0.943)
  Pallas kernels: 31.7 us -> 30.5 us
  local copies, waits for them, and re-layouts: 0.66 us -> 0 us
    unnamed x4 -> x0, local copies, waits for them, and re-layouts: 0.66 us -> none
    pallas_call x1, Pallas kernels: 29 us -> 28.4 us  [fused(): pl.pallas_call(functools.partial(exchange_kernel, kv_count, head_count),...]
    pallas_call x1, Pallas kernels: 2.68 us -> 2.13 us  [fused(): pl.pallas_call(write_kernel, out_shape=(jax.ShapeDtypeStruct((seq_count,...]
where the time goes in v4:
time: 31.3 us; the launch traced here: 31.2 us
  Pallas kernels  30.5 us (97%)
  between operations  0.65 us (2%)
    pallas_call x1, Pallas kernels, fused(): pl.pallas_call(functools.partial(exchange_kernel, kv_count, head_count),...  28.4 us
    pallas_call x1, Pallas kernels, fused(): pl.pallas_call(write_kernel, out_shape=(jax.ShapeDtypeStruct((seq_count,...  2.13 us

profile of v4, /device:TPU:0, one launch (start us, length us, event | category | flops | bytes accessed | tf_op | source)
XLA Modules:
  0.0 31.2 jit_solution(4493965161606308425)
XLA Ops:
  0.6 28.4 %exchange.1 = (s32[4,8,128]{2,1,0:T(8,128)S(1)}, f32[4,24,256]{2,1,0:T(8,128)S(1)}, bf16[4,2,24,512]{3,2,1,0:T(8,128)(2,1)S(1)}, f32[4,8,128]{2,1,0:T(8,128)S(1)...) custom-call(s32[4]{0:T(128)} %lengths_ref.1, s32[4]{0:T(128)} %accepted_ref.1, ...), custom_call_target="tpu_custom_call" | custom-call | tf_op jit(solution)/shard_map/exchange/pallas_call | solution.py:685
  29.0 2.1 %write.1 = (f32[4,24,256]{2,1,0:T(8,128)}, bf16[4,256,512]{2,1,0:T(8,128)(2,1)}, bf16[4,256,512]{2,1,0:T(8,128)(2,1)}, f32[4,8,256]{2,1,0:T(8,128)}) custom-call(s32[4,8,128]{2,1,0:T(8,128)S(1)} %get-tuple-element.11.valid_ref, f32[4,24,256]{2,1,0:T(8,128)S(1)} %get-tuple-element.12.mixed_ref, bf16[4,2,24,512]{3,2,1,0:T(8,128)(2,1)S(1)} %get-tuple-element.13.fresh_ref, ...), custom_call_target="tpu_custom_call" | custom-call | tf_op jit(solution)/shard_map/write/pallas_call | solution.py:708
